TPU v7x, 128 devices: a whole 4x4x4 slice. The times are simulated.
128 devices in a mesh: ep: 64 (over z, y, x), tp: 2 (over core).
Axes of the slice: x: 4, y: 4, z: 4, core: 2. Of those that a mesh axis runs over, the one named last changes fastest.
Arguments:
- tokens: bfloat16 [2048, 2048], P('ep'), may hold values from -6 to 6
- lengths: int32 [2048], P('ep'), may hold values from 128 to 1024
- key_cache: bfloat16 [2048, 1024, 256], P('ep', None, 'tp'), may hold values from -1000 to 1000
- value_cache: bfloat16 [2048, 1024, 256], P('ep', None, 'tp'), may hold values from -6 to 6
- gate_cache: float32 [2048, 16, 1024], P('ep', 'tp'), may hold values from -130 to 0, as said below
- mix_gain: float32 [2048], replicated, may hold values from 0.1 to 1.9
- query_weight: bfloat16 [2048, 1024], P(None, 'tp'), may hold values from -0.125 to 0.125
- key_weight: bfloat16 [2048, 256], P(None, 'tp'), may hold values from -0.125 to 0.125
- value_weight: bfloat16 [2048, 256], P(None, 'tp'), may hold values from -0.125 to 0.125
- forget_weight: bfloat16 [2048, 16], P(None, 'tp'), may hold values from -0.125 to 0.125
- out_weight: bfloat16 [1024, 2048], P('tp'), may hold values from -0.1875 to 0.1875
- expert_gain: float32 [2048], replicated, may hold values from 0.1 to 1.9
- routes: int32 [2048, 2], P('ep'), may hold values from 0 to 7, all different within a row; in each aligned block of 32 rows (0 to 31, 32 to 63, ...) at most 12 rows name the same one
- route_weights: float32 [2048, 2], P('ep'), may hold values from 0.2 to 1
- expert_gate: bfloat16 [2048, 65536], P(None, ('ep', 'tp')), may hold values from -0.125 to 0.125
- expert_up: bfloat16 [2048, 65536], P(None, ('ep', 'tp')), may hold values from -0.125 to 0.125
- expert_down: bfloat16 [65536, 2048], P(('ep', 'tp')), may hold values from -0.0625 to 0.0625
Outputs:
- layer_out: bfloat16 [2048, 2048], P('ep')
Inputs may be any that keep to these rules, and one draw needn't show every extreme that they name: `routes`: within the rows of one index of ep, no expert is named more than 12 times, and in every draw some expert is named exactly 12 times in some such rows; the 2 experts of a row differ. `gate_cache`: for each sequence and head the values never rise along the cache positions.
All inputs are finite; a program needn't handle non-finite values.
Results may differ from a plain program's by a relative error of at most 0.013.
Values may be sent and summed in bfloat16 or wider, within the bound.
A program may use at most 128 MiB of HBM per device.

v0:
```python
import jax
import jax.numpy as jnp
from jax import lax
from jax.sharding import PartitionSpec as P

HD = 64
EXPERTS = 8
CAP = 12


eps = 1e-06


def sent_to_all(x, axis):
    copies = jnp.broadcast_to(x, (lax.axis_size(axis), *x.shape))
    return lax.all_to_all(copies, axis, split_axis=0, concat_axis=0, tiled=True)


def of_everyone(x, axis):
    return sent_to_all(x, axis).astype(jnp.float32).sum(axis=0)


def cut_along(x, dim, size):
    before, after = (x.shape[:dim], x.shape[dim + 1 :])
    return jnp.moveaxis(x.reshape(*before, size, -1, *after), dim, 0)


def sent_and_summed(x, axis, dim):
    size = lax.axis_size(axis)
    tiles = lax.all_to_all(cut_along(x, dim, size), axis, 0, 0, tiled=True)
    return jnp.sum(tiles.astype(jnp.float32), axis=0)


def in_order(tiles, dim):
    dims = list(tiles.shape[1:])
    dims[dim] *= tiles.shape[0]
    return jnp.moveaxis(tiles, 0, dim).reshape(dims)


def collect(x, axis, dim):
    tiles = sent_to_all(x, axis)
    return in_order(tiles, dim)


def normed(values, gain):
    floats = values.astype(jnp.float32)
    return floats * lax.rsqrt(jnp.mean(floats * floats, axis=-1, keepdims=True) + eps) * gain


def attend(queries, key_new, value_new, log_gate, key_rows, value_rows, cumulative, length):
    seq_count, head_count, head_size = queries.shape
    kv_count = key_new.shape[1]
    group_size = head_count // kv_count
    cache_locations = key_rows.shape[1]
    factor = head_size ** (-0.5)
    grouped = queries.reshape(seq_count, kv_count, group_size, head_size)
    key_split = key_rows.reshape(seq_count, cache_locations, kv_count, head_size)
    value_split = value_rows.reshape(seq_count, cache_locations, kv_count, head_size)
    scores = (
        jnp.einsum(
            "skgd,spkd->skgp", grouped, key_split, preferred_element_type=jnp.float32
        ).reshape(seq_count, head_count, cache_locations)
        * factor
    )
    positions = jnp.arange(cache_locations, dtype=jnp.int32)
    latest = jnp.sum(
        jnp.where(positions[None, None, :] == (length - 1)[:, None, None], cumulative, 0.0), axis=-1
    )
    scores = scores + (latest + log_gate)[..., None] - cumulative
    valid = positions[None, None, :] < length[:, None, None]
    scores = jnp.where(valid, scores, -jnp.inf)
    own_score = (
        jnp.einsum("skgd,skd->skg", grouped, key_new, preferred_element_type=jnp.float32).reshape(
            seq_count, head_count
        )
        * factor
    )
    highest = jnp.maximum(jnp.max(scores, axis=-1), own_score)
    raised = jnp.exp(scores - highest[..., None])
    own_raised = jnp.exp(own_score - highest)
    denominator = jnp.sum(raised, axis=-1) + own_raised
    weights = (raised / denominator[..., None]).astype(jnp.bfloat16)
    own_weight = (own_raised / denominator).astype(jnp.bfloat16)
    mixed = jnp.einsum(
        "skgp,spkd->skgd",
        weights.reshape(seq_count, kv_count, group_size, cache_locations),
        value_split,
        preferred_element_type=jnp.float32,
    )
    mixed = (
        mixed
        + own_weight.reshape(seq_count, kv_count, group_size)[..., None].astype(jnp.float32)
        * value_new.astype(jnp.float32)[:, :, None, :]
    )
    return mixed.reshape(seq_count, head_count * head_size).astype(jnp.bfloat16)


def expert_work(rows_in, expert_gate, expert_up, expert_down):
    leading = rows_in.shape[:-1]
    flat_rows = rows_in.reshape(-1, rows_in.shape[-1])
    gate_out = jnp.dot(flat_rows, expert_gate, preferred_element_type=jnp.float32)
    up_out = jnp.dot(flat_rows, expert_up, preferred_element_type=jnp.float32)
    hidden = (jax.nn.silu(gate_out) * up_out).astype(jnp.bfloat16)
    return jnp.dot(hidden, expert_down, preferred_element_type=jnp.float32).reshape(
        leading + (expert_down.shape[1],)
    )


def combine(returned, target, route_weights):
    capacity = returned.shape[1]
    columns = returned.shape[2]
    blocks = jnp.sum(
        returned.reshape(EXPERTS, -1, capacity, columns).astype(jnp.float32), axis=1
    ).reshape(EXPERTS * capacity, columns)
    picked = jnp.take(blocks, target, axis=0).reshape(route_weights.shape + (columns,))
    return jnp.sum(picked * route_weights[..., None], axis=1)


def on_device(
    tokens,
    lengths,
    key_cache,
    value_cache,
    gate_cache,
    mix_gain,
    query_weight,
    key_weight,
    value_weight,
    forget_weight,
    out_weight,
    expert_gain,
    routes,
    route_weights,
    expert_gate,
    expert_up,
    expert_down,
):
    seq_count = tokens.shape[0]
    width = tokens.shape[1]
    normal_in = normed(tokens, mix_gain).astype(jnp.bfloat16)
    queries = (
        jnp.dot(normal_in, query_weight, preferred_element_type=jnp.float32)
        .astype(jnp.bfloat16)
        .reshape(seq_count, -1, HD)
    )
    key_new = (
        jnp.dot(normal_in, key_weight, preferred_element_type=jnp.float32)
        .astype(jnp.bfloat16)
        .reshape(seq_count, -1, HD)
    )
    value_new = (
        jnp.dot(normal_in, value_weight, preferred_element_type=jnp.float32)
        .astype(jnp.bfloat16)
        .reshape(seq_count, -1, HD)
    )
    log_gate = jax.nn.log_sigmoid(
        jnp.dot(normal_in, forget_weight, preferred_element_type=jnp.float32)
    )
    mixed = attend(
        queries, key_new, value_new, log_gate, key_cache, value_cache, gate_cache, lengths
    )
    partial_out = jnp.dot(mixed, out_weight, preferred_element_type=jnp.float32).astype(
        jnp.bfloat16
    )
    residual = (
        tokens.astype(jnp.float32) + of_everyone(partial_out, "tp").astype(jnp.float32)
    ).astype(jnp.bfloat16)
    expert_in = normed(residual, expert_gain).astype(jnp.bfloat16)
    top_count = routes.shape[1]
    flat_routes = routes.reshape(-1)
    one_hot = (flat_routes[:, None] == jnp.arange(EXPERTS, dtype=jnp.int32)[None, :]).astype(
        jnp.int32
    )
    slot_index = jnp.sum((jnp.cumsum(one_hot, axis=0) - 1) * one_hot, axis=1)
    target = flat_routes * CAP + slot_index
    dispatch = (jnp.arange(EXPERTS * CAP, dtype=jnp.int32)[:, None] == target[None, :]).astype(
        jnp.bfloat16
    )
    repeated = jnp.repeat(expert_in, top_count, axis=0)
    outgoing = jnp.dot(dispatch, repeated, preferred_element_type=jnp.float32).astype(jnp.bfloat16)
    pieces = lax.axis_size("ep") // EXPERTS
    outgoing = jnp.broadcast_to(
        outgoing.reshape(EXPERTS, 1, CAP, width), (EXPERTS, pieces, CAP, width)
    ).reshape(EXPERTS * pieces, CAP, width)
    half_width = width // lax.axis_size("tp")
    start = lax.axis_index("tp") * half_width
    outgoing_half = lax.dynamic_slice_in_dim(outgoing, start, half_width, 2)
    full_rows = lax.all_gather(
        lax.all_to_all(outgoing_half, "ep", split_axis=0, concat_axis=0, tiled=True),
        "tp",
        axis=2,
        tiled=True,
    )
    partial_rows = expert_work(full_rows, expert_gate, expert_up, expert_down).astype(jnp.bfloat16)
    share = sent_and_summed(partial_rows, "tp", 2).astype(jnp.bfloat16)
    returned = lax.all_to_all(share, "ep", split_axis=0, concat_axis=0, tiled=True)
    mixture = combine(returned, target, route_weights)
    own_half = lax.dynamic_slice_in_dim(residual, start, half_width, 1).astype(jnp.float32)
    return collect((own_half + mixture).astype(jnp.bfloat16), "tp", 1)


def solution(mesh):
    return jax.shard_map(
        on_device,
        mesh=mesh,
        in_specs=(
            P("ep", None),
            P("ep"),
            P("ep", None, "tp"),
            P("ep", None, "tp"),
            P("ep", "tp", None),
            P(),
            P(None, "tp"),
            P(None, "tp"),
            P(None, "tp"),
            P(None, "tp"),
            P("tp", None),
            P(),
            P("ep", None),
            P("ep", None),
            P(None, ("ep", "tp")),
            P(None, ("ep", "tp")),
            P(("ep", "tp"), None),
        ),
        out_specs=P("ep", None),
        check_vma=False,
    )
```

profile of v0, /device:TPU:1, one launch (start us, length us, event | category | flops | bytes accessed | tf_op | source)
XLA Modules:
  0.0 223.7 jit_solution(6335412211523638819)
XLA Ops:
  6.5 0.8 broadcast_add_fusion
  7.3 0.7 iota_compare_fusion.1
  8.1 1.0 fusion.6
  9.1 2.2 convolution_convert_fusion.3
  11.3 0.1 reshape_reshape.3
  11.5 11.9 %copy.122 = bf16[32,1024,128]{1,2,0:T(8,128)(2,1)} copy(bf16[32,1024,128]{2,1,0:T(8,128)(2,1)} %param.19) | data formatting | bytes 16777216 | tf_op args[2]
  23.4 4.6 %convolution_multiply_fusion = f32[32,2,4,1024]{3,2,1,0:T(4,128)S(1)} fusion(bf16[32,2,4,64]{3,2,1,0:T(4,128)(2,1)S(1)} %reshape_reshape.3, bf16[32,1024,2,64]{1,3,2,0:T(8,128)(2,1)} %bitcast.43), kind=kOutput, calls=%fused_computation.7 | convolution fusion | flops 33816576 | bytes 9469952 | tf_op jit(solution)/shard_map/skgd,spkd->skgp/dot_general | solution.py:60
  28.0 1.4 mul.132
  29.4 0.1 iota_compare_fusion
  29.4 1.5 select_reduce_fusion
  31.0 0.2 fusion.14
  31.3 1.9 fusion.24
  33.3 1.3 convolution_convert_fusion.5
  34.6 0.1 reshape.214
  34.7 0.2 fusion.25
  34.9 0.1 copy.144
  35.1 0.3 fusion.2
  35.5 1.1 divide_convert_fusion
  36.6 1.2 reshape.193
  37.9 0.1 copy.132
  38.0 1.3 fusion.1
  39.3 0.1 reshape.201
  39.4 11.9 %copy.129 = bf16[32,1024,128]{1,2,0:T(8,128)(2,1)} copy(bf16[32,1024,128]{2,1,0:T(8,128)(2,1)} %param.20) | data formatting | bytes 16777216 | tf_op args[3]
  51.3 5.6 %fusion = bf16[32,2,4,64]{3,2,1,0:T(4,128)(2,1)S(1)} fusion(bf16[32,2,4,1024]{3,2,1,0:T(4,128)(2,1)S(1)} %reshape.193, bf16[32,1024,2,64]{1,3,2,0:T(8,128)(2,1)} %bitcast.46, f32[32,2,64]{2,1,0:T(2,128)S(1)} %reshape.201, f32[32,2,4]{2,1,0:T(2,128)S(1)} %copy.132), kind=kOutput, calls=%fused_computation.9 | convolution fusion | flops 33603584 | bytes 8963072 | tf_op jit(solution)/shard_map/skgp,spkd->skgd/dot_general | solution.py:84
  57.0 0.1 convert_element_type.100
  57.1 2.1 convolution_convert_fusion.2
  59.2 0.7 broadcast_in_dim.66
  59.9 4.8 %all-to-all-start = ((bf16[2,32,2048]{2,1,0:T(8,128)(2,1)}), bf16[2,32,2048]{2,1,0:T(8,128)(2,1)S(1)}, u32[]{:S(2)}, u32[]{:S(2)}) async-start(bf16[2,32,2048]{2,1,0:T(8,128)(2,1)} %broadcast_in_dim.66), calls=%async_computation | async-start | bytes 524288 | tf_op jit(solution)/shard_map/all_to_all | solution.py:16
  64.7 1.2 all-to-all-done
  65.9 0.2 fusion.3
  66.1 0.1 fusion.5
  66.2 0.1 broadcast_in_dim.68
  66.4 0.1 reshape.196
  66.5 0.1 copy.133
  66.6 0.1 reshape.195
  66.8 0.1 reduce_window_sum.11
  66.9 0.2 select_reduce_fusion.1
  67.0 0.3 convolution_convert_fusion.1
  67.3 0.1 broadcast_in_dim.69
  67.4 0.5 broadcast_in_dim.70
  68.0 0.2 constant_dynamic-slice_fusion
  68.1 40.1 %all_to_all.25 = bf16[64,12,1024]{2,1,0:T(8,128)(2,1)} all-to-all(bf16[64,12,1024]{2,1,0:T(8,128)(2,1)S(1)} %constant_dynamic-slice_fusion), channel_id=1, replica_groups=mesh['ep'=64,'tp'=2] {'ep'}, dimensions={0} | all-to-all | bytes 3145728 | tf_op jit(solution)/shard_map/all_to_all | solution.py:189
  108.3 15.0 %all-gather.2.cloned.1.call-done = bf16[64,12,2048]{2,1,0:T(8,128)(2,1)} async-done(((bf16[64,12,1024]{2,1,0:T(8,128)(2,1)}), bf16[64,12,2048]{2,1,0:T(8,128)(2,1)}) %all-gather.2.cloned.1.call-update) | async-done | bytes 3145744 | tf_op jit(solution)/shard_map/all_gather | solution.py:188
  123.3 6.2 %reshape.198 = bf16[768,2048]{1,0:T(8,128)(2,1)} reshape(bf16[64,12,2048]{2,1,0:T(8,128)(2,1)} %all-gather.2.cloned.1.call-done) | data formatting | bytes 6291456 | tf_op jit(solution)/shard_map/reshape | solution.py:100
  129.5 5.5 %fusion.26 = f32[768,512]{1,0:T(8,128)} fusion(bf16[768,2048]{1,0:T(8,128)(2,1)} %reshape.198, bf16[2048,512]{1,0:T(8,128)(2,1)} %param.31), kind=kOutput, calls=%fused_computation.67 | convolution fusion | flops 1610612736 | bytes 6815744 | tf_op jit(solution)/shard_map/dot_general | solution.py:101
  135.0 8.2 %convolution_convert_fusion = bf16[768,2048]{1,0:T(8,128)(2,1)} fusion(bf16[512,2048]{1,0:T(8,128)(2,1)S(1)} %copy-done, f32[768,512]{1,0:T(8,128)} %fusion.26, bf16[768,2048]{1,0:T(8,128)(2,1)} %reshape.198, bf16[2048,512]{1,0:T(8,128)(2,1)} %param.32), kind=kOutput, calls=%fused_computation.2 | convolution fusion | flops 3225157632 | bytes 12058624 | tf_op jit(solution)/shard_map/dot_general | solution.py:104
  143.1 6.1 %convert_element_type.111 = bf16[64,12,2,1024]{3,2,1,0:T(2,128)(2,1)} reshape(bf16[768,2048]{1,0:T(8,128)(2,1)} %convolution_convert_fusion) | data formatting | bytes 6291456 | tf_op jit(solution)/shard_map/convert_element_type | solution.py:194
  149.3 3.6 %copy.148 = bf16[64,12,2,1024]{3,0,1,2:T(8,128)(2,1)S(1)} copy(bf16[64,12,2,1024]{3,2,1,0:T(2,128)(2,1)} %convert_element_type.111) | data formatting | bytes 6291456 | tf_op jit(solution)/shard_map/convert_element_type | solution.py:194
  152.9 7.1 %all_to_all.26 = bf16[2,64,12,1024]{3,1,2,0:T(8,128)(2,1)} all-to-all(bf16[2,64,12,1024]{3,1,2,0:T(8,128)(2,1)S(1)} %bitcast.44), channel_id=1, replica_groups=mesh['ep'=64,'tp'=2] {'tp'}, dimensions={0} | all-to-all | bytes 6291456 | tf_op jit(solution)/shard_map/all_to_all | solution.py:30
  160.0 4.2 %reduce_sum.98 = bf16[64,12,1024]{2,0,1:T(8,128)(2,1)} reduce(bf16[2,64,12,1024]{3,1,2,0:T(8,128)(2,1)} %all_to_all.26, bf16[]{:T(256)} %constant.55.clone.1), dimensions={0}, to_apply=%region_8.9 | reduce | flops 786432 | bytes 4718594 | tf_op jit(solution)/shard_map/reduce_sum | solution.py:31
  164.2 3.7 %copy.137 = bf16[64,12,1024]{2,1,0:T(8,128)(2,1)} copy(bf16[64,12,1024]{2,0,1:T(8,128)(2,1)} %reduce_sum.98) | data formatting | bytes 3145728 | tf_op jit(solution)/shard_map/reduce_sum | solution.py:31
  167.9 10.5 %all-to-all-start.3 = ((bf16[64,12,1024]{2,1,0:T(8,128)(2,1)}), bf16[64,12,1024]{2,1,0:T(8,128)(2,1)}, u32[]{:S(2)}, u32[]{:S(2)}) async-start(bf16[64,12,1024]{2,1,0:T(8,128)(2,1)} %copy.137), calls=%async_computation.3 | async-start | bytes 4194304 | tf_op jit(solution)/shard_map/all_to_all | solution.py:196
  178.4 0.1 reduce_sum.96
  178.5 0.1 copy.140
  178.6 0.1 mul.152
  178.8 0.1 copy.135
  178.9 0.1 copy.141
  179.0 28.2 %all-to-all-done.3 = bf16[64,12,1024]{2,1,0:T(8,128)(2,1)} async-done(((bf16[64,12,1024]{2,1,0:T(8,128)(2,1)}), bf16[64,12,1024]{2,1,0:T(8,128)(2,1)}, u32[]{:S(2)}, u32[]{:S(2)}) %all-to-all-start.3) | async-done | bytes 1572896 | tf_op jit(solution)/shard_map/all_to_all | solution.py:196
  207.2 2.0 convert_reduce_fusion
  209.3 0.7 gather_fusion
  210.0 0.1 gather.7
  210.2 0.5 multiply_reduce_fusion
  210.7 5.5 %all_to_all.27 = bf16[2,32,1024]{2,1,0:T(8,128)(2,1)S(1)} all-to-all(bf16[2,32,1024]{2,1,0:T(8,128)(2,1)S(1)} %broadcast_in_dim.72), channel_id=1, replica_groups=mesh['ep'=64,'tp'=2] {'tp'}, dimensions={0} | all-to-all | bytes 262144 | tf_op jit(solution)/shard_map/all_to_all | solution.py:16
  216.2 0.7 copy.146
  (39 shorter events, 0.8 us)
Async XLA Ops:
  6.5 128.4 %copy-start = (bf16[512,2048]{1,0:T(8,128)(2,1)S(1)}, bf16[512,2048]{1,0:T(8,128)(2,1)}, u32[]{:S(2)}) copy-start(bf16[512,2048]{1,0:T(8,128)(2,1)} %param.33) | copy-start | bytes 6291460
  28.0 3.0 %copy-start.1 = (bf16[32,2048]{1,0:T(8,128)(2,1)S(1)}, bf16[32,2048]{1,0:T(8,128)(2,1)}, u32[]{:S(2)}) copy-start(bf16[32,2048]{1,0:T(8,128)(2,1)} %param.17) | copy-start | bytes 393220
  28.0 3.0 %copy-start.2 = (f32[2048]{0:T(1024)S(1)}, f32[2048]{0:T(1024)}, u32[]{:S(2)}) copy-start(f32[2048]{0:T(1024)} %param.22) | copy-start | bytes 24580
  28.0 3.0 %copy-start.6 = (bf16[2048,8]{0,1:T(8,128)(2,1)S(1)}, bf16[2048,8]{0,1:T(8,128)(2,1)}, u32[]{:S(2)}) copy-start(bf16[2048,8]{0,1:T(8,128)(2,1)} %param.26) | copy-start | bytes 98308
  57.1 9.0 %copy-start.4 = (f32[2048]{0:T(1024)S(1)}, f32[2048]{0:T(1024)}, u32[]{:S(2)}) copy-start(f32[2048]{0:T(1024)} %param.28) | copy-start | bytes 24580
  59.2 7.3 %copy-start.3 = (s32[32,2]{0,1:T(2,128)S(1)}, s32[32,2]{0,1:T(2,128)}, u32[]{:S(2)}) copy-start(s32[32,2]{0,1:T(2,128)} %param.29) | copy-start | bytes 772
  59.9 6.0 %all-to-all-start = ((bf16[2,32,2048]{2,1,0:T(8,128)(2,1)}), bf16[2,32,2048]{2,1,0:T(8,128)(2,1)S(1)}, u32[]{:S(2)}, u32[]{:S(2)}) async-start(bf16[2,32,2048]{2,1,0:T(8,128)(2,1)} %broadcast_in_dim.66), calls=%async_computation | async-start | bytes 524288 | tf_op jit(solution)/shard_map/all_to_all | solution.py:16
  64.7 58.6 %all-gather.2.cloned.1.call-start = ((), (), s32[]{:S(2)}) async-start(), calls=%async_computation.5 | async-start | bytes 6291456 | tf_op jit(solution)/shard_map/all_gather | solution.py:188
  167.9 11.0 %copy-start.5 = (f32[32,2]{0,1:T(2,128)S(1)}, f32[32,2]{0,1:T(2,128)}, u32[]{:S(2)}) copy-start(f32[32,2]{0,1:T(2,128)} %param.30) | copy-start | bytes 772
  167.9 39.3 %all-to-all-start.3 = ((bf16[64,12,1024]{2,1,0:T(8,128)(2,1)}), bf16[64,12,1024]{2,1,0:T(8,128)(2,1)}, u32[]{:S(2)}, u32[]{:S(2)}) async-start(bf16[64,12,1024]{2,1,0:T(8,128)(2,1)} %copy.137), calls=%async_computation.3 | async-start | bytes 4194304 | tf_op jit(solution)/shard_map/all_to_all | solution.py:196
Sparse Core Ops, SparseCore 0:
  108.4 14.8 all-gather.1
where the time goes:
time: 225 us; the launch traced here: 224 us
  blocking collectives  52.8 us (23%)
  local copies, waits for them, and re-layouts  51.2 us (23%)
  waiting for transfers between devices  44.4 us (20%)
  matrix products  31.4 us (14%)
  starting transfers between devices  15.3 us (7%)
  other arithmetic  14.9 us (7%)
  between operations  13.7 us (6%)
    all_to_all x1, blocking collectives, on_device(): lax.all_to_all(outgoing_half, 'ep', split_axis=0, concat_axis=0, tiled=True)  40.1 us
    all_to_all x1, waiting for transfers between devices, on_device(): lax.all_to_all(share, 'ep', split_axis=0, concat_axis=0, tiled=True)  28.2 us
    unnamed x18, local copies, waits for them, and re-layouts  24.1 us
    all_gather x1, waiting for transfers between devices, on_device(): lax.all_gather(lax.all_to_all(outgoing_half, 'ep', split_axis=0, concat_a...  15 us
    all_to_all x1, starting transfers between devices, on_device(): lax.all_to_all(share, 'ep', split_axis=0, concat_axis=0, tiled=True)  10.5 us
    convert_element_type x2, local copies, waits for them, and re-layouts, on_device(): expert_work(full_rows, expert_gate, expert_up, expert_down)  9.75 us
    dot_general x1, matrix products, expert_work(): jnp.dot(hidden, expert_down, preferred_element_type=jnp.float32)  8.18 us
    all_to_all x1, blocking collectives, sent_and_summed(): tiles = lax.all_to_all(cut_along(x, dim, size), axis, 0, 0, tiled=True)  7.09 us
  transfers between devices with their start and end apart: 3, of which 3 were waited for; matrix products, arithmetic and copies ran while one was open for 0% of the time, Pallas kernels for 0%

commit v1 on v0

--- a/solution.py
+++ b/solution.py
@@ -1,7 +1,137 @@
+import functools
 import jax
 import jax.numpy as jnp
 from jax import lax
+from jax.experimental import pallas as pl
+from jax.experimental.pallas import tpu as pltpu
 from jax.sharding import PartitionSpec as P
+
+SEQS = 32
+POS = 1024
+LANES = 128
+HEADS_HERE = 8
+
+
+def rms(values, gain):
+    return values * lax.rsqrt(jnp.mean(values * values, axis=-1, keepdims=True) + 1e-06) * gain
+
+
+def attention_kernel(
+    len_ref, tok_hbm, key_hbm, value_hbm, gate_hbm, gain_hbm, wq_hbm, wk_hbm, wv_hbm, wf_hbm, wo_hbm,
+    out_ref,
+    tok, gain, wq, wk, wv, wf, wo, keys, values, gates, qs, owns, lgs, vnew, mixed, sems, kv_sems,
+):
+    blocks, per = kv_sems.shape[1], SEQS // kv_sems.shape[1]
+    small = [(tok_hbm, tok), (gain_hbm, gain), (wq_hbm, wq), (wk_hbm, wk), (wv_hbm, wv), (wf_hbm, wf), (wo_hbm, wo)]
+    copies = [pltpu.make_async_copy(a, b, sems.at[i]) for i, (a, b) in enumerate(small)]
+
+    def block_copies(b):
+        rows = pl.ds(b * per, per)
+        return [
+            pltpu.make_async_copy(src.at[rows], dst.at[rows], kv_sems.at[i, b])
+            for i, (src, dst) in enumerate(((key_hbm, keys), (gate_hbm, gates), (value_hbm, values)))
+        ]
+
+    for c in copies[:6]:
+        c.start()
+    for b in range(blocks):
+        for c in block_copies(b):
+            c.start()
+    copies[6].start()
+
+    copies[0].wait()
+    copies[1].wait()
+    ni = rms(tok[...].astype(jnp.float32), gain[...]).astype(jnp.bfloat16)
+    lane = lax.broadcasted_iota(jnp.int32, (SEQS, LANES), 1)
+    left = lane < 64
+    for c in copies[2:6]:
+        c.wait()
+    dot = functools.partial(jnp.dot, preferred_element_type=jnp.float32)
+    q = dot(ni, wq[...]).astype(jnp.bfloat16).astype(jnp.float32) * 0.125
+    kn = dot(ni, wk[...]).astype(jnp.bfloat16).astype(jnp.float32)
+    vnew[...] = dot(ni, wv[...]).astype(jnp.bfloat16).astype(jnp.float32)
+    f = dot(ni, wf[...])
+    lg = jnp.minimum(f, 0.0) - jnp.log1p(jnp.exp(-jnp.abs(f)))
+    for h in range(HEADS_HERE):
+        column = q[:, 128 * (h // 2) : 128 * (h // 2) + 128]
+        if h % 2 != h // 4:
+            column = pltpu.roll(column, 64, 1)
+        column = jnp.where(left if h < 4 else ~left, column, 0.0)
+        rows = pl.ds(h, SEQS, stride=HEADS_HERE)
+        qs[rows, :] = column
+        owns[rows, :] = jnp.broadcast_to(jnp.sum(column * kn, axis=1, keepdims=True), (SEQS, LANES))
+        lgs[rows, :] = jnp.broadcast_to(lg[:, h : h + 1], (SEQS, LANES))
+
+    position = lax.broadcasted_iota(jnp.int32, (HEADS_HERE, POS), 1)
+
+    def block(b, carry):
+        for c in block_copies(b):
+            c.wait()
+        for j in range(per):
+            s = b * per + j
+            rows = pl.ds(s * HEADS_HERE, HEADS_HERE)
+            length = len_ref[s]
+            g = gates[s]
+            score = lax.dot_general(
+                qs[rows, :].astype(jnp.bfloat16), keys[s], (((1,), (1,)), ((), ())),
+                preferred_element_type=jnp.float32,
+            )
+            latest = jnp.sum(jnp.where(position == length - 1, g, 0.0), axis=1, keepdims=True)
+            own = owns[rows, 0:1]
+            score = jnp.where(position < length, score + (latest + lgs[rows, 0:1]) - g, -jnp.inf)
+            top = jnp.maximum(jnp.max(score, axis=1, keepdims=True), own)
+            raised = jnp.exp(score - top)
+            own_raised = jnp.exp(own - top)
+            total = jnp.sum(raised, axis=1, keepdims=True) + own_raised
+            o = dot(raised.astype(jnp.bfloat16), values[s])
+            mixed[rows, :] = (o + own_raised * vnew[pl.ds(s, 1), :]) / total
+        return carry
+
+    lax.fori_loop(0, blocks, block, 0)
+    parts = []
+    for c in range(4):
+        pair = []
+        for h in (2 * c, 2 * c + 1):
+            o = mixed[pl.ds(h, SEQS, stride=HEADS_HERE), :]
+            pair.append(pltpu.roll(o, 64, 1) if h % 2 != h // 4 else o)
+        parts.append(jnp.where(left, pair[0], pair[1]).astype(jnp.bfloat16))
+    copies[6].wait()
+    out_ref[...] = dot(jnp.concatenate(parts, axis=1), wo[...]).astype(jnp.bfloat16)
+
+
+def attention(tokens, lengths, key_cache, value_cache, gate_cache, gain, wq, wk, wv, wf, wo, blocks=8):
+    width = tokens.shape[1]
+    f32, bf16 = jnp.float32, jnp.bfloat16
+    any_space = pl.BlockSpec(memory_space=pl.ANY)
+    return pl.pallas_call(
+        attention_kernel,
+        out_shape=jax.ShapeDtypeStruct((SEQS, width), bf16),
+        in_specs=[pl.BlockSpec(memory_space=pltpu.SMEM)] + [any_space] * 10,
+        out_specs=pl.BlockSpec(memory_space=pltpu.VMEM),
+        scratch_shapes=[
+            pltpu.VMEM((SEQS, width), bf16),
+            pltpu.VMEM((1, width), f32),
+            pltpu.VMEM(wq.shape, bf16),
+            pltpu.VMEM(wk.shape, bf16),
+            pltpu.VMEM(wv.shape, bf16),
+            pltpu.VMEM(wf.shape, bf16),
+            pltpu.VMEM(wo.shape, bf16),
+            pltpu.VMEM(key_cache.shape, bf16),
+            pltpu.VMEM(value_cache.shape, bf16),
+            pltpu.VMEM(gate_cache.shape, f32),
+            pltpu.VMEM((SEQS * HEADS_HERE, LANES), f32),
+            pltpu.VMEM((SEQS * HEADS_HERE, LANES), f32),
+            pltpu.VMEM((SEQS * HEADS_HERE, LANES), f32),
+            pltpu.VMEM((SEQS, LANES), f32),
+            pltpu.VMEM((SEQS * HEADS_HERE, LANES), f32),
+            pltpu.SemaphoreType.DMA((7,)),
+            pltpu.SemaphoreType.DMA((3, blocks)),
+        ],
+        compiler_params=pltpu.CompilerParams(vmem_limit_bytes=40 * 1024 * 1024),
+        cost_estimate=pl.CostEstimate(flops=500_000_000, bytes_accessed=24_000_000, transcendentals=300_000),
+        name="attention",
+    )(lengths, tokens, key_cache, value_cache, gate_cache, gain.reshape(1, width), wq, wk, wv, wf, wo)
+
 
 HD = 64
 EXPERTS = 8
@@ -45,54 +175,6 @@
 def normed(values, gain):
     floats = values.astype(jnp.float32)
     return floats * lax.rsqrt(jnp.mean(floats * floats, axis=-1, keepdims=True) + eps) * gain
-
-
-def attend(queries, key_new, value_new, log_gate, key_rows, value_rows, cumulative, length):
-    seq_count, head_count, head_size = queries.shape
-    kv_count = key_new.shape[1]
-    group_size = head_count // kv_count
-    cache_locations = key_rows.shape[1]
-    factor = head_size ** (-0.5)
-    grouped = queries.reshape(seq_count, kv_count, group_size, head_size)
-    key_split = key_rows.reshape(seq_count, cache_locations, kv_count, head_size)
-    value_split = value_rows.reshape(seq_count, cache_locations, kv_count, head_size)
-    scores = (
-        jnp.einsum(
-            "skgd,spkd->skgp", grouped, key_split, preferred_element_type=jnp.float32
-        ).reshape(seq_count, head_count, cache_locations)
-        * factor
-    )
-    positions = jnp.arange(cache_locations, dtype=jnp.int32)
-    latest = jnp.sum(
-        jnp.where(positions[None, None, :] == (length - 1)[:, None, None], cumulative, 0.0), axis=-1
-    )
-    scores = scores + (latest + log_gate)[..., None] - cumulative
-    valid = positions[None, None, :] < length[:, None, None]
-    scores = jnp.where(valid, scores, -jnp.inf)
-    own_score = (
-        jnp.einsum("skgd,skd->skg", grouped, key_new, preferred_element_type=jnp.float32).reshape(
-            seq_count, head_count
-        )
-        * factor
-    )
-    highest = jnp.maximum(jnp.max(scores, axis=-1), own_score)
-    raised = jnp.exp(scores - highest[..., None])
-    own_raised = jnp.exp(own_score - highest)
-    denominator = jnp.sum(raised, axis=-1) + own_raised
-    weights = (raised / denominator[..., None]).astype(jnp.bfloat16)
-    own_weight = (own_raised / denominator).astype(jnp.bfloat16)
-    mixed = jnp.einsum(
-        "skgp,spkd->skgd",
-        weights.reshape(seq_count, kv_count, group_size, cache_locations),
-        value_split,
-        preferred_element_type=jnp.float32,
-    )
-    mixed = (
-        mixed
-        + own_weight.reshape(seq_count, kv_count, group_size)[..., None].astype(jnp.float32)
-        * value_new.astype(jnp.float32)[:, :, None, :]
-    )
-    return mixed.reshape(seq_count, head_count * head_size).astype(jnp.bfloat16)
 
 
 def expert_work(rows_in, expert_gate, expert_up, expert_down):
@@ -135,32 +217,10 @@
     expert_up,
     expert_down,
 ):
-    seq_count = tokens.shape[0]
     width = tokens.shape[1]
-    normal_in = normed(tokens, mix_gain).astype(jnp.bfloat16)
-    queries = (
-        jnp.dot(normal_in, query_weight, preferred_element_type=jnp.float32)
-        .astype(jnp.bfloat16)
-        .reshape(seq_count, -1, HD)
-    )
-    key_new = (
-        jnp.dot(normal_in, key_weight, preferred_element_type=jnp.float32)
-        .astype(jnp.bfloat16)
-        .reshape(seq_count, -1, HD)
-    )
-    value_new = (
-        jnp.dot(normal_in, value_weight, preferred_element_type=jnp.float32)
-        .astype(jnp.bfloat16)
-        .reshape(seq_count, -1, HD)
-    )
-    log_gate = jax.nn.log_sigmoid(
-        jnp.dot(normal_in, forget_weight, preferred_element_type=jnp.float32)
-    )
-    mixed = attend(
-        queries, key_new, value_new, log_gate, key_cache, value_cache, gate_cache, lengths
-    )
-    partial_out = jnp.dot(mixed, out_weight, preferred_element_type=jnp.float32).astype(
-        jnp.bfloat16
+    partial_out = attention(
+        tokens, lengths, key_cache, value_cache, gate_cache, mix_gain,
+        query_weight, key_weight, value_weight, forget_weight, out_weight,
     )
     residual = (
         tokens.astype(jnp.float32) + of_everyone(partial_out, "tp").astype(jnp.float32)

time: 225 us -> 190 us (0.84)
  local copies, waits for them, and re-layouts: 51.2 us -> 30.3 us
  matrix products: 31.4 us -> 13.9 us
  Pallas kernels: 0 us -> 17 us
  other arithmetic: 14.9 us -> 3.85 us
    dot_general x8 -> x0, matrix products: 17.5 us -> none  [the longest x1 5.65 us: attend(): jnp.einsum('skgp,spkd->skgd', weights.reshape(seq_count, kv_count, group_...]
    pallas_call x0 -> x1, Pallas kernels: none -> 17 us  [attention(): pl.pallas_call(attention_kernel, out_shape=jax.ShapeDtypeStruct((SEQS, wi...]
    unnamed x18 -> x31, local copies, waits for them, and re-layouts: 24.1 us -> 10.1 us
    convert_element_type x2, local copies, waits for them, and re-layouts: 9.75 us -> 6.49 us  [on_device(): expert_work(full_rows, expert_gate, expert_up, expert_down)]
  transfers between devices with their start and end apart: 3 -> 3, of which waited for: 3 -> 3; matrix products, arithmetic and copies ran while one was open for 0% -> 1% of each run, Pallas kernels for 0% -> 0%
where the time goes in v1:
time: 190 us
  blocking collectives  51.8 us (27%)
  waiting for transfers between devices  44.1 us (23%)
  local copies, waits for them, and re-layouts  30.3 us (16%)
  Pallas kernels  17 us (9%)
  starting transfers between devices  15.1 us (8%)
  matrix products  13.9 us (7%)
  between operations  13.6 us (7%)
  other arithmetic  3.85 us (2%)
    all_to_all x1, blocking collectives, on_device(): lax.all_to_all(outgoing_half, 'ep', split_axis=0, concat_axis=0, tiled=True)  40.1 us
    all_to_all x1, waiting for transfers between devices, on_device(): lax.all_to_all(share, 'ep', split_axis=0, concat_axis=0, tiled=True)  28.4 us
    pallas_call x1, Pallas kernels, attention(): pl.pallas_call(attention_kernel, out_shape=jax.ShapeDtypeStruct((SEQS, wi...  17 us
    all_gather x1, waiting for transfers between devices, on_device(): lax.all_gather(lax.all_to_all(outgoing_half, 'ep', split_axis=0, concat_a...  15 us
    all_to_all x1, starting transfers between devices, on_device(): lax.all_to_all(share, 'ep', split_axis=0, concat_axis=0, tiled=True)  10.3 us
    unnamed x31, local copies, waits for them, and re-layouts  10.1 us
    dot_general x1, matrix products, expert_work(): jnp.dot(hidden, expert_down, preferred_element_type=jnp.float32)  8.16 us
    convert_element_type x2, local copies, waits for them, and re-layouts, on_device(): expert_work(full_rows, expert_gate, expert_up, expert_down)  6.49 us
  transfers between devices with their start and end apart: 3, of which 3 were waited for; matrix products, arithmetic and copies ran while one was open for 1% of the time, Pallas kernels for 0%

profile of v1, /device:TPU:1, one launch (start us, length us, event | category | flops | bytes accessed | tf_op | source)
XLA Modules:
  0.0 189.6 jit_solution(3469954805543781790)
XLA Ops:
  6.5 0.0 copy-start
  6.5 1.2 copy.67.wf_hbm
  7.7 0.0 copy-start.2
  7.7 1.6 copy-done.2
  9.3 0.0 copy-start.3
  9.3 1.6 copy-done.3
  10.9 1.2 copy-done.4
  12.1 0.0 copy-start.5
  12.1 0.9 copy-done.5
  13.0 1.0 copy-done.7
  14.1 1.0 copy-done.8
  15.1 0.7 copy-done.9
  15.8 0.7 copy-done.10
  16.5 17.0 %attention.1 = bf16[32,2048]{1,0:T(8,128)(2,1)S(1)} custom-call(s32[32]{0:T(128)S(1)} %copy-done.10, bf16[32,2048]{1,0:T(8,128)(2,1)S(1)} %copy-done.5, bf16[32,1024,128]{2,1,0:T(8,128)(2,1)} %key_hbm.1, bf16[32,1024,128]{2,1,0:T(8,128)(2,1)} %value_hbm.1, f32[32,8,1024]{2,1,0:T(8,128)S(1)} %copy-done.4, f32[1,2048]{1,0:T(1,128)S(1)} %bitcast.23, ...), custom_call_target="tpu_custom_call" | custom-call | flops 500000000 | bytes 24000000 | tf_op jit(solution)/shard_map/attention/pallas_call | solution.py:106
  33.5 0.0 copy-start.12
  33.5 0.7 broadcast_in_dim.32
  34.2 4.8 %all-to-all-start = ((bf16[2,32,2048]{2,1,0:T(8,128)(2,1)}), bf16[2,32,2048]{2,1,0:T(8,128)(2,1)S(1)}, u32[]{:S(2)}, u32[]{:S(2)}) async-start(bf16[2,32,2048]{2,1,0:T(8,128)(2,1)} %broadcast_in_dim.32), calls=%async_computation | async-start | bytes 524288 | tf_op jit(solution)/shard_map/all_to_all | solution.py:146
  39.0 0.0 all-gather.2.cloned.1.call-start
  39.0 0.0 copy-done.11
  39.0 0.1 copy.68
  39.1 0.1 reshape.92
  39.2 0.1 fusion.3
  39.3 0.1 reduce_window_sum.11
  39.4 0.2 select_reduce_fusion
  39.6 0.6 all-to-all-done
  40.2 0.0 copy-done.6
  40.2 0.2 fusion
  40.4 0.0 copy-done.12
  40.4 0.1 fusion.2
  40.5 0.1 broadcast_in_dim.34
  40.7 0.1 reshape.93
  40.8 0.2 convolution_convert_fusion.1
  41.0 0.1 broadcast_in_dim.35
  41.1 0.5 broadcast_in_dim.36
  41.7 0.2 constant_dynamic-slice_fusion
  41.9 40.1 %all_to_all.25 = bf16[64,12,1024]{2,1,0:T(8,128)(2,1)} all-to-all(bf16[64,12,1024]{2,1,0:T(8,128)(2,1)S(1)} %constant_dynamic-slice_fusion), channel_id=1, replica_groups=mesh['ep'=64,'tp'=2] {'ep'}, dimensions={0} | all-to-all | bytes 3145728 | tf_op jit(solution)/shard_map/all_to_all | solution.py:249
  82.0 0.0 all-gather.2.cloned.1.call-update
  82.0 15.0 %all-gather.2.cloned.1.call-done = bf16[64,12,2048]{2,1,0:T(8,128)(2,1)} async-done(((bf16[64,12,1024]{2,1,0:T(8,128)(2,1)}), bf16[64,12,2048]{2,1,0:T(8,128)(2,1)}) %all-gather.2.cloned.1.call-update) | async-done | bytes 3145744 | tf_op jit(solution)/shard_map/all_gather | solution.py:248
  97.0 6.2 %reshape.95 = bf16[768,2048]{1,0:T(8,128)(2,1)} reshape(bf16[64,12,2048]{2,1,0:T(8,128)(2,1)} %all-gather.2.cloned.1.call-done) | data formatting | bytes 6291456 | tf_op jit(solution)/shard_map/reshape | solution.py:182
  103.2 5.5 %fusion.7 = f32[768,512]{1,0:T(8,128)} fusion(bf16[768,2048]{1,0:T(8,128)(2,1)} %reshape.95, bf16[2048,512]{1,0:T(8,128)(2,1)} %param.31), kind=kOutput, calls=%fused_computation.31 | convolution fusion | flops 1610612736 | bytes 6815744 | tf_op jit(solution)/shard_map/dot_general | solution.py:183
  108.7 0.0 copy-done
  108.7 8.2 %convolution_convert_fusion = bf16[768,2048]{1,0:T(8,128)(2,1)} fusion(bf16[512,2048]{1,0:T(8,128)(2,1)S(1)} %copy-done, f32[768,512]{1,0:T(8,128)} %fusion.7, bf16[768,2048]{1,0:T(8,128)(2,1)} %reshape.95, bf16[2048,512]{1,0:T(8,128)(2,1)} %param.32), kind=kOutput, calls=%fused_computation.2 | convolution fusion | flops 3225157632 | bytes 12058624 | tf_op jit(solution)/shard_map/dot_general | solution.py:186
  116.9 4.8 %convert_element_type.56 = bf16[64,12,2,1024]{3,2,1,0:T(2,128)(2,1)S(1)} reshape(bf16[768,2048]{1,0:T(8,128)(2,1)} %convolution_convert_fusion) | data formatting | bytes 6291456 | tf_op jit(solution)/shard_map/convert_element_type | solution.py:254
  121.6 1.7 copy.81
  123.4 6.2 %all_to_all.26 = bf16[2,64,12,1024]{3,1,2,0:T(8,128)(2,1)S(1)} all-to-all(bf16[2,64,12,1024]{3,1,2,0:T(8,128)(2,1)S(1)} %bitcast.24), channel_id=1, replica_groups=mesh['ep'=64,'tp'=2] {'tp'}, dimensions={0} | all-to-all | bytes 6291456 | tf_op jit(solution)/shard_map/all_to_all | solution.py:160
  129.5 2.3 %reduce_sum.65 = bf16[64,12,1024]{2,0,1:T(8,128)(2,1)} reduce(bf16[2,64,12,1024]{3,1,2,0:T(8,128)(2,1)S(1)} %all_to_all.26, bf16[]{:T(256)} %constant.44.clone.1), dimensions={0}, to_apply=%region_4.5 | reduce | flops 786432 | bytes 4718594 | tf_op jit(solution)/shard_map/reduce_sum | solution.py:161
  131.8 3.6 %copy.72 = bf16[64,12,1024]{2,1,0:T(8,128)(2,1)} copy(bf16[64,12,1024]{2,0,1:T(8,128)(2,1)} %reduce_sum.65) | data formatting | bytes 3145728 | tf_op jit(solution)/shard_map/reduce_sum | solution.py:161
  135.5 10.3 %all-to-all-start.3 = ((bf16[64,12,1024]{2,1,0:T(8,128)(2,1)}), bf16[64,12,1024]{2,1,0:T(8,128)(2,1)S(1)}, u32[]{:S(2)}, u32[]{:S(2)}) async-start(bf16[64,12,1024]{2,1,0:T(8,128)(2,1)} %copy.72), calls=%async_computation.3 | async-start | bytes 4194304 | tf_op jit(solution)/shard_map/all_to_all | solution.py:256
  145.7 0.1 reduce_sum.63
  145.8 0.1 copy.75
  145.9 0.1 mul.80
  146.0 0.1 copy.69
  146.1 0.1 copy.70
  146.2 0.0 copy-done.13
  146.2 0.1 copy.76
  146.3 28.4 %all-to-all-done.3 = bf16[64,12,1024]{2,1,0:T(8,128)(2,1)S(1)} async-done(((bf16[64,12,1024]{2,1,0:T(8,128)(2,1)}), bf16[64,12,1024]{2,1,0:T(8,128)(2,1)S(1)}, u32[]{:S(2)}, u32[]{:S(2)}) %all-to-all-start.3) | async-done | bytes 1572896 | tf_op jit(solution)/shard_map/all_to_all | solution.py:256
  174.8 0.4 convert_reduce_fusion
  175.1 0.0 copy-start.1
  175.2 0.7 gather_fusion
  175.9 0.1 gather.7
  176.1 0.5 multiply_reduce_fusion
  176.6 5.5 %all_to_all.27 = bf16[2,32,1024]{2,1,0:T(8,128)(2,1)S(1)} all-to-all(bf16[2,32,1024]{2,1,0:T(8,128)(2,1)S(1)} %broadcast_in_dim.38), channel_id=1, replica_groups=mesh['ep'=64,'tp'=2] {'tp'}, dimensions={0} | all-to-all | bytes 262144 | tf_op jit(solution)/shard_map/all_to_all | solution.py:146
  182.1 0.7 copy.79
  182.7 0.0 copy-done.1
  (18 shorter events, 0.2 us)
Async XLA Ops:
  6.5 102.2 %copy-start = (bf16[512,2048]{1,0:T(8,128)(2,1)S(1)}, bf16[512,2048]{1,0:T(8,128)(2,1)}, u32[]{:S(2)}) copy-start(bf16[512,2048]{1,0:T(8,128)(2,1)} %param.33) | copy-start | bytes 6291460
  7.7 1.6 copy-start.2
  9.3 1.6 copy-start.3
  10.9 1.2 copy-start.4
  12.1 0.9 copy-start.5
  13.0 1.0 copy-start.7
  14.1 1.0 copy-start.8
  15.1 0.7 copy-start.9
  15.8 0.7 copy-start.10
  16.5 22.5 %copy-start.11 = (s32[32,2]{0,1:T(2,128)S(1)}, s32[32,2]{0,1:T(2,128)}, u32[]{:S(2)}) copy-start(s32[32,2]{0,1:T(2,128)} %param.29) | copy-start | bytes 772
  16.5 23.8 %copy-start.6 = (bf16[32,2048]{1,0:T(8,128)(2,1)S(1)}, bf16[32,2048]{1,0:T(8,128)(2,1)}, u32[]{:S(2)}) copy-start(bf16[32,2048]{1,0:T(8,128)(2,1)} %tok_hbm.1) | copy-start | bytes 393220
  33.5 6.9 %copy-start.12 = (f32[2048]{0:T(1024)S(1)}, f32[2048]{0:T(1024)}, u32[]{:S(2)}) copy-start(f32[2048]{0:T(1024)} %param.28) | copy-start | bytes 24580
  34.2 6.0 %all-to-all-start = ((bf16[2,32,2048]{2,1,0:T(8,128)(2,1)}), bf16[2,32,2048]{2,1,0:T(8,128)(2,1)S(1)}, u32[]{:S(2)}, u32[]{:S(2)}) async-start(bf16[2,32,2048]{2,1,0:T(8,128)(2,1)} %broadcast_in_dim.32), calls=%async_computation | async-start | bytes 524288 | tf_op jit(solution)/shard_map/all_to_all | solution.py:146
  39.0 58.0 %all-gather.2.cloned.1.call-start = ((), (), s32[]{:S(2)}) async-start(), calls=%async_computation.5 | async-start | bytes 6291456 | tf_op jit(solution)/shard_map/all_gather | solution.py:248
  135.5 10.8 %copy-start.13 = (f32[32,2]{0,1:T(2,128)S(1)}, f32[32,2]{0,1:T(2,128)}, u32[]{:S(2)}) copy-start(f32[32,2]{0,1:T(2,128)} %param.30) | copy-start | bytes 772
  135.5 39.3 %all-to-all-start.3 = ((bf16[64,12,1024]{2,1,0:T(8,128)(2,1)}), bf16[64,12,1024]{2,1,0:T(8,128)(2,1)S(1)}, u32[]{:S(2)}, u32[]{:S(2)}) async-start(bf16[64,12,1024]{2,1,0:T(8,128)(2,1)} %copy.72), calls=%async_computation.3 | async-start | bytes 4194304 | tf_op jit(solution)/shard_map/all_to_all | solution.py:256
  175.1 7.6 %copy-start.1 = (bf16[512,2048]{1,0:T(8,128)(2,1)S(1)}, bf16[512,2048]{1,0:T(8,128)(2,1)}, u32[]{:S(2)}) copy-start(bf16[512,2048]{1,0:T(8,128)(2,1)} %param.33) | copy-start | bytes 6291460
Sparse Core Ops, SparseCore 0:
  82.2 14.8 all-gather.1

commit v2 on v1

--- a/solution.py
+++ b/solution.py
@@ -127,136 +127,292 @@
             pltpu.SemaphoreType.DMA((7,)),
             pltpu.SemaphoreType.DMA((3, blocks)),
         ],
-        compiler_params=pltpu.CompilerParams(vmem_limit_bytes=40 * 1024 * 1024),
+        compiler_params=pltpu.CompilerParams(vmem_limit_bytes=60 * 1024 * 1024),
         cost_estimate=pl.CostEstimate(flops=500_000_000, bytes_accessed=24_000_000, transcendentals=300_000),
         name="attention",
     )(lengths, tokens, key_cache, value_cache, gate_cache, gain.reshape(1, width), wq, wk, wv, wf, wo)
 
 
-HD = 64
-EXPERTS = 8
+MESH = pl.DeviceIdType.MESH
 CAP = 12
-
-
-eps = 1e-06
-
-
-def sent_to_all(x, axis):
-    copies = jnp.broadcast_to(x, (lax.axis_size(axis), *x.shape))
-    return lax.all_to_all(copies, axis, split_axis=0, concat_axis=0, tiled=True)
-
-
-def of_everyone(x, axis):
-    return sent_to_all(x, axis).astype(jnp.float32).sum(axis=0)
-
-
-def cut_along(x, dim, size):
-    before, after = (x.shape[:dim], x.shape[dim + 1 :])
-    return jnp.moveaxis(x.reshape(*before, size, -1, *after), dim, 0)
-
-
-def sent_and_summed(x, axis, dim):
-    size = lax.axis_size(axis)
-    tiles = lax.all_to_all(cut_along(x, dim, size), axis, 0, 0, tiled=True)
-    return jnp.sum(tiles.astype(jnp.float32), axis=0)
-
-
-def in_order(tiles, dim):
-    dims = list(tiles.shape[1:])
-    dims[dim] *= tiles.shape[0]
-    return jnp.moveaxis(tiles, 0, dim).reshape(dims)
-
-
-def collect(x, axis, dim):
-    tiles = sent_to_all(x, axis)
-    return in_order(tiles, dim)
-
-
-def normed(values, gain):
-    floats = values.astype(jnp.float32)
-    return floats * lax.rsqrt(jnp.mean(floats * floats, axis=-1, keepdims=True) + eps) * gain
-
-
-def expert_work(rows_in, expert_gate, expert_up, expert_down):
-    leading = rows_in.shape[:-1]
-    flat_rows = rows_in.reshape(-1, rows_in.shape[-1])
-    gate_out = jnp.dot(flat_rows, expert_gate, preferred_element_type=jnp.float32)
-    up_out = jnp.dot(flat_rows, expert_up, preferred_element_type=jnp.float32)
-    hidden = (jax.nn.silu(gate_out) * up_out).astype(jnp.bfloat16)
-    return jnp.dot(hidden, expert_down, preferred_element_type=jnp.float32).reshape(
-        leading + (expert_down.shape[1],)
-    )
-
-
-def combine(returned, target, route_weights):
-    capacity = returned.shape[1]
-    columns = returned.shape[2]
-    blocks = jnp.sum(
-        returned.reshape(EXPERTS, -1, capacity, columns).astype(jnp.float32), axis=1
-    ).reshape(EXPERTS * capacity, columns)
-    picked = jnp.take(blocks, target, axis=0).reshape(route_weights.shape + (columns,))
-    return jnp.sum(picked * route_weights[..., None], axis=1)
+HALF = 1024
+BLOCK = 48
+CHUNK = 4 * BLOCK
+
+
+def moe_kernel(
+    part_ref, tok_ref, gain_ref, routes_ref, rw_ref, wg_hbm, wu_hbm, wd_hbm,
+    out_ref,
+    wg, wu, wd, other_part, res, xe, wts, wtg, xg, cross_out, xf,
+    pm, po, pi, ys, ry, zs_out, rxo, rxc, c_out, rc, cf_out, rr, rb, u_out, ur, fo,
+    wsem, ss, rs,
+):
+    f32, bf16 = jnp.float32, jnp.bfloat16
+    dot = functools.partial(jnp.dot, preferred_element_type=f32)
+    e, t = lax.axis_index("ep"), lax.axis_index("tp")
+    z, y, x = e // 16, lax.rem(e // 4, 4), lax.rem(e, 4)
+    g = y // 2
+
+    def chip(zz, yy, xx):
+        return (zz * 16 + yy * 4 + xx, t)
+
+    partner = (e, 1 - t)
+    z_peer = {k: chip(jnp.bitwise_xor(z, k), y, x) for k in (1, 2, 3)}
+    x_peer = {k: chip(z, y, jnp.bitwise_xor(x, k)) for k in (1, 2, 3)}
+    y_peer = chip(z, jnp.bitwise_xor(y, 1), x)
+    y_cross = chip(z, 3 - y, x)
+    near = (1, 3, 2)
+
+    loads = [
+        pltpu.make_async_copy(wg_hbm, wg, wsem.at[0]),
+        pltpu.make_async_copy(wu_hbm, wu, wsem.at[1]),
+        pltpu.make_async_copy(wd_hbm.at[:, pl.ds(0, HALF)], wd.at[0], wsem.at[2]),
+        pltpu.make_async_copy(wd_hbm.at[:, pl.ds(HALF, HALF)], wd.at[1], wsem.at[3]),
+    ]
+    for c in loads:
+        c.start()
+
+    count = [0]
+    started = []
+
+    def send(src, dst, device):
+        i = count[0]
+        count[0] += 1
+        c = pltpu.make_async_remote_copy(
+            src_ref=src, dst_ref=dst, send_sem=ss.at[i], recv_sem=rs.at[i], device_id=device, device_id_type=MESH
+        )
+        c.start()
+        started.append(c)
+        return c
+
+    barrier = pltpu.get_barrier_semaphore()
+    peers = [partner, y_peer, y_cross, *z_peer.values(), *x_peer.values()]
+    for p in peers:
+        pl.semaphore_signal(barrier, inc=1, device_id=p, device_id_type=MESH)
+
+    rows = tok_ref.shape[0]
+    lane = lax.broadcasted_iota(jnp.int32, (rows, LANES), 1)
+    upper = lane >= 64
+    sub = jnp.where(upper, lane - 64, lane)
+    owner = lax.shift_right_logical(sub * 43, 9)
+    slot = sub - CAP * owner
+    mine = (sub < 4 * CAP) & (owner == z)
+    which = jnp.where(upper, 1 - g, g)
+    r0, r1 = routes_ref[:, 0:1], routes_ref[:, 1:2]
+    w0, w1 = rw_ref[:, 0:1], rw_ref[:, 1:2]
+    before = (
+        lax.broadcasted_iota(jnp.int32, (rows, rows), 1) < lax.broadcasted_iota(jnp.int32, (rows, rows), 0)
+    ).astype(f32).astype(bf16)
+    for k in range(4):
+        expert = 2 * jnp.bitwise_xor(z, k) + which
+        named = jnp.where((r0 == expert) | (r1 == expert), 1.0, 0.0).astype(bf16)
+        earlier = dot(before, named)
+        here = mine & (named.astype(f32) > 0.5) & (earlier == slot.astype(f32))
+        wts[k] = jnp.where(here, jnp.where(r0 == expert, w0, w1), 0.0)
+    wtg[0] = wts[0]
+
+    pl.semaphore_wait(barrier, len(peers))
+    c_part = send(part_ref, other_part, partner)
+    c_wt = {k: send(wts.at[k], wtg.at[k], z_peer[k]) for k in near}
+
+    c_part.wait_recv()
+    total = tok_ref[...].astype(f32) + (part_ref[...].astype(f32) + other_part[...].astype(f32))
+    res_b = total.astype(bf16)
+    res[0] = res_b[:, :HALF]
+    res[1] = res_b[:, HALF:]
+    expert_in = rms(res_b.astype(f32), gain_ref[...]).astype(bf16)
+    xe[0] = expert_in[:, :HALF]
+    xe[1] = expert_in[:, HALF:]
+    xg[0] = xe[t]
+    c_x = {k: send(xg.at[0], xg.at[k], z_peer[k]) for k in near}
+    for k in near:
+        c_wt[k].wait_recv()
+    for k in near:
+        c_x[k].wait_recv()
+
+    weights = wtg[...].reshape(4 * rows, LANES)
+    picks = jnp.where(weights > 0.0, 1.0, 0.0).astype(bf16)
+    packed = lax.dot_general(
+        picks, xg[...].reshape(4 * rows, HALF), (((0,), (0,)), ((), ())), preferred_element_type=f32
+    ).astype(bf16)
+    xf[t, 0, 0] = packed[0:BLOCK]
+    cross_out[...] = packed[64 : 64 + BLOCK]
+
+    mine_at = lambda d, q: xf.at[t, d, q]
+    fwd = {}
+
+    def forward(d, q):
+        fwd[d, q] = send(mine_at(d, q), mine_at(d, q), partner)
+
+    c_cross = send(cross_out, mine_at(0, 2), y_cross)
+    c_ax = {d: send(mine_at(0, 0), mine_at(d, 0), x_peer[d]) for d in near}
+    c_ay = {0: send(mine_at(0, 0), mine_at(0, 1), y_peer)}
+    forward(0, 0)
+    c_cross.wait_recv()
+    c_by = send(mine_at(0, 2), mine_at(0, 3), y_peer)
+    c_bx = {(d, 2): send(mine_at(0, 2), mine_at(d, 2), x_peer[d]) for d in near}
+    forward(0, 2)
+    for d in (1, 3):
+        c_ax[d].wait_recv()
+        c_ay[d] = send(mine_at(d, 0), mine_at(d, 1), y_peer)
+        forward(d, 0)
+    c_ay[0].wait_recv()
+    forward(0, 1)
+    c_by.wait_recv()
+    for d in near:
+        c_bx[d, 3] = send(mine_at(0, 3), mine_at(d, 3), x_peer[d])
+    forward(0, 3)
+    c_ax[2].wait_recv()
+    c_ay[2] = send(mine_at(2, 0), mine_at(2, 1), y_peer)
+    forward(2, 0)
+
+    for c in loads:
+        c.wait()
+    c_pi = {}
+
+    def compute(d):
+        for q in range(4):
+            fwd[d, q].wait_recv()
+        x0, x1 = xf[0, d].reshape(CHUNK, HALF), xf[1, d].reshape(CHUNK, HALF)
+        gate = dot(x0, wg[0:HALF]) + dot(x1, wg[HALF : 2 * HALF])
+        up = dot(x0, wu[0:HALF]) + dot(x1, wu[HALF : 2 * HALF])
+        hidden = (gate / (1.0 + jnp.exp(-gate)) * up).astype(bf16)
+        po[d] = dot(hidden, wd[1 - t]).astype(bf16)
+        c_pi[d] = send(po.at[d], pi.at[d], partner)
+        pm[d] = dot(hidden, wd[t])
+
+    c_ry, c_xc, c_xo = {}, {}, {}
+
+    def arrive(d):
+        c_bx[d, 2].wait_recv()
+        forward(d, 2)
+        c_ay[d].wait_recv()
+        forward(d, 1)
+        c_bx[d, 3].wait_recv()
+        forward(d, 3)
+
+    def finish(d):
+        c_pi[d].wait_recv()
+        ys[d] = (pm[d] + pi[d].astype(f32)).astype(bf16).reshape(4, BLOCK, HALF)
+        if d:
+            c_xc[d] = send(ys.at[d, pl.ds(2, 2)], rxc.at[d], x_peer[d])
+        c_ry[d] = send(ys.at[d, 1], ry.at[d], y_peer)
+
+    def second(d):
+        c_ry[d].wait_recv()
+        zs_out[d] = (ys[d, 0].astype(f32) + ry[d].astype(f32)).astype(bf16)
+        if d:
+            c_xo[d] = send(zs_out.at[d], rxo.at[d], x_peer[d])
+
+    compute(0)
+    arrive(1)
+    compute(1)
+    finish(0)
+    arrive(3)
+    compute(3)
+    finish(1)
+    second(0)
+    arrive(2)
+    compute(2)
+    finish(3)
+    second(1)
+    finish(2)
+    second(3)
+    second(2)
+
+    for d in near:
+        c_xc[d].wait_recv()
+    crossed = ys[0, 2:4].astype(f32) + rxc[1].astype(f32) + rxc[3].astype(f32) + rxc[2].astype(f32)
+    c_out[...] = crossed[1].astype(bf16)
+    c_rc = send(c_out, rc, y_peer)
+    for d in near:
+        c_xo[d].wait_recv()
+    own = zs_out[0].astype(f32) + rxo[1].astype(f32) + rxo[3].astype(f32) + rxo[2].astype(f32)
+    rb[...] = jnp.zeros(rb.shape, bf16)
+    rb[0:BLOCK] = own.astype(bf16)
+    c_rc.wait_recv()
+    cf_out[...] = (crossed[0] + rc[...].astype(f32)).astype(bf16)
+    c_rr = send(cf_out, rr, y_cross)
+    high = weights.astype(bf16)
+    low = (weights - high.astype(f32)).astype(bf16)
+    c_rr.wait_recv()
+    rb[64 : 64 + BLOCK] = rr[...]
+    back = dot(high, rb[...]) + dot(low, rb[...])
+    u_out[...] = back.astype(bf16).reshape(4, rows, HALF)
+    c_u = {k: send(u_out.at[k], ur.at[k], z_peer[k]) for k in near}
+    mixture = res[t].astype(f32) + back[0:rows]
+    for k in near:
+        c_u[k].wait_recv()
+    mixture = mixture + ur[1].astype(f32) + ur[2].astype(f32) + ur[3].astype(f32)
+    fo[t] = mixture.astype(bf16)
+    c_fo = send(fo.at[t], fo.at[t], partner)
+    c_fo.wait_recv()
+    out_ref[:, 0:HALF] = fo[0]
+    out_ref[:, HALF : 2 * HALF] = fo[1]
+    for c in started:
+        c.wait_send()
+
+
+def moe(partial_out, tokens, gain, routes, route_weights, wg, wu, wd):
+    rows, width = tokens.shape
+    f32, bf16 = jnp.float32, jnp.bfloat16
+    any_space = pl.BlockSpec(memory_space=pl.ANY)
+    vmem = pl.BlockSpec(memory_space=pltpu.VMEM)
+    blocks = lambda *s: pltpu.VMEM((*s, BLOCK, HALF), bf16)
+    return pl.pallas_call(
+        moe_kernel,
+        out_shape=jax.ShapeDtypeStruct((rows, width), bf16),
+        in_specs=[vmem] * 5 + [any_space] * 3,
+        out_specs=vmem,
+        scratch_shapes=[
+            pltpu.VMEM(wg.shape, bf16),
+            pltpu.VMEM(wu.shape, bf16),
+            pltpu.VMEM((2, wd.shape[0], HALF), bf16),
+            pltpu.VMEM((rows, width), bf16),
+            pltpu.VMEM((2, rows, HALF), bf16),
+            pltpu.VMEM((2, rows, HALF), bf16),
+            pltpu.VMEM((4, rows, LANES), f32),
+            pltpu.VMEM((4, rows, LANES), f32),
+            pltpu.VMEM((4, rows, HALF), bf16),
+            blocks(),
+            blocks(2, 4, 4),
+            pltpu.VMEM((4, CHUNK, HALF), f32),
+            pltpu.VMEM((4, CHUNK, HALF), bf16),
+            pltpu.VMEM((4, CHUNK, HALF), bf16),
+            blocks(4, 4),
+            blocks(4),
+            blocks(4),
+            blocks(4),
+            blocks(4, 2),
+            blocks(),
+            blocks(),
+            blocks(),
+            blocks(),
+            pltpu.VMEM((LANES, HALF), bf16),
+            pltpu.VMEM((4, rows, HALF), bf16),
+            pltpu.VMEM((4, rows, HALF), bf16),
+            pltpu.VMEM((2, rows, HALF), bf16),
+            pltpu.SemaphoreType.DMA((4,)),
+            pltpu.SemaphoreType.DMA((64,)),
+            pltpu.SemaphoreType.DMA((64,)),
+        ],
+        compiler_params=pltpu.CompilerParams(
+            collective_id=0, has_side_effects=True, vmem_limit_bytes=56 * 1024 * 1024
+        ),
+        cost_estimate=pl.CostEstimate(flops=5_000_000_000, bytes_accessed=8_000_000, transcendentals=400_000),
+        name="routed_experts",
+    )(partial_out, tokens, gain.reshape(1, width), routes, route_weights, wg, wu, wd)
 
 
 def on_device(
-    tokens,
-    lengths,
-    key_cache,
-    value_cache,
-    gate_cache,
-    mix_gain,
-    query_weight,
-    key_weight,
-    value_weight,
-    forget_weight,
-    out_weight,
-    expert_gain,
-    routes,
-    route_weights,
-    expert_gate,
-    expert_up,
-    expert_down,
+    tokens, lengths, key_cache, value_cache, gate_cache, mix_gain, query_weight, key_weight, value_weight,
+    forget_weight, out_weight, expert_gain, routes, route_weights, expert_gate, expert_up, expert_down,
 ):
-    width = tokens.shape[1]
     partial_out = attention(
         tokens, lengths, key_cache, value_cache, gate_cache, mix_gain,
         query_weight, key_weight, value_weight, forget_weight, out_weight,
     )
-    residual = (
-        tokens.astype(jnp.float32) + of_everyone(partial_out, "tp").astype(jnp.float32)
-    ).astype(jnp.bfloat16)
-    expert_in = normed(residual, expert_gain).astype(jnp.bfloat16)
-    top_count = routes.shape[1]
-    flat_routes = routes.reshape(-1)
-    one_hot = (flat_routes[:, None] == jnp.arange(EXPERTS, dtype=jnp.int32)[None, :]).astype(
-        jnp.int32
-    )
-    slot_index = jnp.sum((jnp.cumsum(one_hot, axis=0) - 1) * one_hot, axis=1)
-    target = flat_routes * CAP + slot_index
-    dispatch = (jnp.arange(EXPERTS * CAP, dtype=jnp.int32)[:, None] == target[None, :]).astype(
-        jnp.bfloat16
-    )
-    repeated = jnp.repeat(expert_in, top_count, axis=0)
-    outgoing = jnp.dot(dispatch, repeated, preferred_element_type=jnp.float32).astype(jnp.bfloat16)
-    pieces = lax.axis_size("ep") // EXPERTS
-    outgoing = jnp.broadcast_to(
-        outgoing.reshape(EXPERTS, 1, CAP, width), (EXPERTS, pieces, CAP, width)
-    ).reshape(EXPERTS * pieces, CAP, width)
-    half_width = width // lax.axis_size("tp")
-    start = lax.axis_index("tp") * half_width
-    outgoing_half = lax.dynamic_slice_in_dim(outgoing, start, half_width, 2)
-    full_rows = lax.all_gather(
-        lax.all_to_all(outgoing_half, "ep", split_axis=0, concat_axis=0, tiled=True),
-        "tp",
-        axis=2,
-        tiled=True,
-    )
-    partial_rows = expert_work(full_rows, expert_gate, expert_up, expert_down).astype(jnp.bfloat16)
-    share = sent_and_summed(partial_rows, "tp", 2).astype(jnp.bfloat16)
-    returned = lax.all_to_all(share, "ep", split_axis=0, concat_axis=0, tiled=True)
-    mixture = combine(returned, target, route_weights)
-    own_half = lax.dynamic_slice_in_dim(residual, start, half_width, 1).astype(jnp.float32)
-    return collect((own_half + mixture).astype(jnp.bfloat16), "tp", 1)
+    return moe(partial_out, tokens, expert_gain, routes, route_weights, expert_gate, expert_up, expert_down)
 
 
 def solution(mesh):

time: 190 us -> 94.5 us (0.50)
  Pallas kernels: 17 us -> 89.6 us
  blocking collectives: 51.8 us -> 0 us
  waiting for transfers between devices: 44.1 us -> 0 us
  local copies, waits for them, and re-layouts: 30.3 us -> 4.7 us
  starting transfers between devices: 15.1 us -> 0 us
  matrix products: 13.9 us -> 0 us
  between operations: 13.6 us -> 0.03 us
  other arithmetic: 3.85 us -> 0 us
    pallas_call x0 -> x1, Pallas kernels: none -> 67 us  [moe(): pl.pallas_call(moe_kernel, out_shape=jax.ShapeDtypeStruct((rows, width),...]
    all_to_all x3 -> x0, blocking collectives: 51.8 us -> none  [the longest x1 40.1 us: on_device(): lax.all_to_all(outgoing_half, 'ep', split_axis=0, concat_axis=0, tiled=True)]
    all_to_all x2 -> x0, waiting for transfers between devices: 29 us -> none  [the longest x1 28.4 us: on_device(): lax.all_to_all(share, 'ep', split_axis=0, concat_axis=0, tiled=True)]
    all_to_all x2 -> x0, starting transfers between devices: 15.1 us -> none  [the longest x1 10.3 us: on_device(): lax.all_to_all(share, 'ep', split_axis=0, concat_axis=0, tiled=True)]
    all_gather x1 -> x0, waiting for transfers between devices: 15 us -> none  [on_device(): lax.all_gather(lax.all_to_all(outgoing_half, 'ep', split_axis=0, concat_a...]
    dot_general x3 -> x0, matrix products: 13.9 us -> none  [the longest x1 8.16 us: expert_work(): jnp.dot(hidden, expert_down, preferred_element_type=jnp.float32)]
    reshape x5 -> x0, local copies, waits for them, and re-layouts: 7.08 us -> none  [the longest x1 6.17 us: expert_work(): flat_rows = rows_in.reshape(-1, rows_in.shape[-1])]
    convert_element_type x2 -> x0, local copies, waits for them, and re-layouts: 6.49 us -> none  [on_device(): expert_work(full_rows, expert_gate, expert_up, expert_down)]
  transfers between devices with their start and end apart: 3 -> 0, of which waited for: 3 -> 0; matrix products, arithmetic and copies ran while one was open for 1% -> 0% of each run, Pallas kernels for 0% -> 0%
where the time goes in v2:
time: 94.5 us; the launch traced here: 94.3 us
  Pallas kernels  89.6 us (95%)
  local copies, waits for them, and re-layouts  4.7 us (5%)
    pallas_call x1, Pallas kernels, moe(): pl.pallas_call(moe_kernel, out_shape=jax.ShapeDtypeStruct((rows, width),...  67 us
    pallas_call x1, Pallas kernels, attention(): pl.pallas_call(attention_kernel, out_shape=jax.ShapeDtypeStruct((SEQS, wi...  22.6 us
    unnamed x8, local copies, waits for them, and re-layouts  4.7 us

profile of v2, /device:TPU:1, one launch (start us, length us, event | category | flops | bytes accessed | tf_op | source)
XLA Modules:
  0.0 94.3 jit_solution(18383951222845283089)
XLA Ops:
  0.0 1.7 %copy.18.wf_hbm = bf16[2048,8]{1,0:T(8,128)(2,1)} copy(bf16[2048,8]{0,1:T(8,128)(2,1)} %param.26) | data formatting | bytes 65536 | tf_op args[9]
  1.7 0.0 copy-start
  1.7 0.0 copy-start.1
  1.8 22.6 %attention.1.part_ref = bf16[32,2048]{1,0:T(8,128)(2,1)} custom-call(s32[32]{0:T(128)} %len_ref.1, bf16[32,2048]{1,0:T(8,128)(2,1)} %tok_ref.1, bf16[32,1024,128]{2,1,0:T(8,128)(2,1)} %key_hbm.1, bf16[32,1024,128]{2,1,0:T(8,128)(2,1)} %value_hbm.1, f32[32,8,1024]{2,1,0:T(8,128)} %gate_hbm.1, f32[1,2048]{1,0:T(1,128)} %bitcast.2, bf16[2048,512]{1,0:T(8,128)(2,1)} %wq_hbm.1, ...), custom_call_target="tpu_custom_call" | custom-call | flops 500000000 | bytes 24000000 | tf_op jit(solution)/shard_map/attention/pallas_call | solution.py:106
  24.4 0.0 copy-done
  24.4 0.7 copy.19.routes_ref
  25.1 0.0 copy-done.1
  25.1 0.7 copy.20.rw_ref
  25.8 67.0 %routed_experts.1 = bf16[32,2048]{1,0:T(8,128)(2,1)} custom-call(bf16[32,2048]{1,0:T(8,128)(2,1)} %attention.1.part_ref, bf16[32,2048]{1,0:T(8,128)(2,1)} %tok_ref.1, f32[1,2048]{1,0:T(1,128)} %bitcast.3, s32[32,2]{1,0:T(8,128)} %copy.19.routes_ref, f32[32,2]{1,0:T(8,128)} %copy.20.rw_ref, bf16[2048,512]{1,0:T(8,128)(2,1)} %wg_hbm.1, ...), custom_call_target="tpu_custom_call" | custom-call | flops 5000000000 | bytes 8000000 | tf_op jit(solution)/shard_map/routed_experts/pallas_call | solution.py:362
  92.8 1.6 %copy.22 = bf16[32,2048]{1,0:T(8,128)(2,1)} copy(bf16[32,2048]{1,0:T(8,128)(2,1)} %routed_experts.1) | data formatting | bytes 262144
Async XLA Ops:
  1.7 22.6 %copy-start = (s32[32,2]{0,1:T(2,128)S(1)}, s32[32,2]{0,1:T(2,128)}, u32[]{:S(2)}) copy-start(s32[32,2]{0,1:T(2,128)} %param.29) | copy-start | bytes 772
  1.7 23.3 %copy-start.1 = (f32[32,2]{0,1:T(2,128)S(1)}, f32[32,2]{0,1:T(2,128)}, u32[]{:S(2)}) copy-start(f32[32,2]{0,1:T(2,128)} %param.30) | copy-start | bytes 772

commit v3 on v2

--- a/solution.py
+++ b/solution.py
@@ -34,23 +34,27 @@
 
     for c in copies[:6]:
         c.start()
-    for b in range(blocks):
+    with jax.named_scope("wait_tok"):
+        copies[0].wait()
+        copies[1].wait()
+    for b in range(2):
+        for c in block_copies(b):
+            c.start()
+    ni = rms(tok[...].astype(jnp.float32), gain[...]).astype(jnp.bfloat16)
+    lane = lax.broadcasted_iota(jnp.int32, (SEQS, LANES), 1)
+    left = lane < 64
+    with jax.named_scope("wait_w"):
+        for c in copies[2:6]:
+            c.wait()
+    for b in range(2, blocks):
         for c in block_copies(b):
             c.start()
     copies[6].start()
-
-    copies[0].wait()
-    copies[1].wait()
-    ni = rms(tok[...].astype(jnp.float32), gain[...]).astype(jnp.bfloat16)
-    lane = lax.broadcasted_iota(jnp.int32, (SEQS, LANES), 1)
-    left = lane < 64
-    for c in copies[2:6]:
-        c.wait()
     dot = functools.partial(jnp.dot, preferred_element_type=jnp.float32)
     q = dot(ni, wq[...]).astype(jnp.bfloat16).astype(jnp.float32) * 0.125
     kn = dot(ni, wk[...]).astype(jnp.bfloat16).astype(jnp.float32)
     vnew[...] = dot(ni, wv[...]).astype(jnp.bfloat16).astype(jnp.float32)
-    f = dot(ni, wf[...])
+    f = lax.dot_general(ni, wf[...], (((1,), (1,)), ((), ())), preferred_element_type=jnp.float32)
     lg = jnp.minimum(f, 0.0) - jnp.log1p(jnp.exp(-jnp.abs(f)))
     for h in range(HEADS_HERE):
         column = q[:, 128 * (h // 2) : 128 * (h // 2) + 128]
@@ -65,8 +69,9 @@
     position = lax.broadcasted_iota(jnp.int32, (HEADS_HERE, POS), 1)
 
     def block(b, carry):
-        for c in block_copies(b):
-            c.wait()
+        with jax.named_scope("wait_kv"):
+            for c in block_copies(b):
+                c.wait()
         for j in range(per):
             s = b * per + j
             rows = pl.ds(s * HEADS_HERE, HEADS_HERE)
@@ -87,7 +92,8 @@
             mixed[rows, :] = (o + own_raised * vnew[pl.ds(s, 1), :]) / total
         return carry
 
-    lax.fori_loop(0, blocks, block, 0)
+    with jax.named_scope("loop"):
+        lax.fori_loop(0, blocks, block, 0)
     parts = []
     for c in range(4):
         pair = []
@@ -95,11 +101,13 @@
             o = mixed[pl.ds(h, SEQS, stride=HEADS_HERE), :]
             pair.append(pltpu.roll(o, 64, 1) if h % 2 != h // 4 else o)
         parts.append(jnp.where(left, pair[0], pair[1]).astype(jnp.bfloat16))
-    copies[6].wait()
+    with jax.named_scope("wait_wo"):
+        copies[6].wait()
     out_ref[...] = dot(jnp.concatenate(parts, axis=1), wo[...]).astype(jnp.bfloat16)
 
 
 def attention(tokens, lengths, key_cache, value_cache, gate_cache, gain, wq, wk, wv, wf, wo, blocks=8):
+    wf = wf.T
     width = tokens.shape[1]
     f32, bf16 = jnp.float32, jnp.bfloat16
     any_space = pl.BlockSpec(memory_space=pl.ANY)
@@ -138,13 +146,14 @@
 HALF = 1024
 BLOCK = 48
 CHUNK = 4 * BLOCK
+AX_ORDER = (1, 3, 2)
 
 
 def moe_kernel(
     part_ref, tok_ref, gain_ref, routes_ref, rw_ref, wg_hbm, wu_hbm, wd_hbm,
     out_ref,
-    wg, wu, wd, other_part, res, xe, wts, wtg, xg, cross_out, xf,
-    pm, po, pi, ys, ry, zs_out, rxo, rxc, c_out, rc, cf_out, rr, rb, u_out, ur, fo,
+    wg, wu, wd, other_part, res, xe, picks, w_high, w_low, pk, sb, xf,
+    pm, po, pi, ys, ry, zs_out, rxo, rxc, c_out, rc, er, rb, fo,
     wsem, ss, rs,
 ):
     f32, bf16 = jnp.float32, jnp.bfloat16
@@ -160,7 +169,7 @@
     z_peer = {k: chip(jnp.bitwise_xor(z, k), y, x) for k in (1, 2, 3)}
     x_peer = {k: chip(z, y, jnp.bitwise_xor(x, k)) for k in (1, 2, 3)}
     y_peer = chip(z, jnp.bitwise_xor(y, 1), x)
-    y_cross = chip(z, 3 - y, x)
+    z_cross = {k: chip(jnp.bitwise_xor(z, k), 3 - y, x) for k in range(4)}
     near = (1, 3, 2)
 
     loads = [
@@ -186,34 +195,35 @@
         return c
 
     barrier = pltpu.get_barrier_semaphore()
-    peers = [partner, y_peer, y_cross, *z_peer.values(), *x_peer.values()]
+    peers = [partner, y_peer, *z_peer.values(), *z_cross.values(), *x_peer.values()]
     for p in peers:
         pl.semaphore_signal(barrier, inc=1, device_id=p, device_id_type=MESH)
 
     rows = tok_ref.shape[0]
     lane = lax.broadcasted_iota(jnp.int32, (rows, LANES), 1)
-    upper = lane >= 64
-    sub = jnp.where(upper, lane - 64, lane)
-    owner = lax.shift_right_logical(sub * 43, 9)
-    slot = sub - CAP * owner
-    mine = (sub < 4 * CAP) & (owner == z)
-    which = jnp.where(upper, 1 - g, g)
-    r0, r1 = routes_ref[:, 0:1], routes_ref[:, 1:2]
-    w0, w1 = rw_ref[:, 0:1], rw_ref[:, 1:2]
-    before = (
-        lax.broadcasted_iota(jnp.int32, (rows, rows), 1) < lax.broadcasted_iota(jnp.int32, (rows, rows), 0)
-    ).astype(f32).astype(bf16)
-    for k in range(4):
-        expert = 2 * jnp.bitwise_xor(z, k) + which
-        named = jnp.where((r0 == expert) | (r1 == expert), 1.0, 0.0).astype(bf16)
-        earlier = dot(before, named)
-        here = mine & (named.astype(f32) > 0.5) & (earlier == slot.astype(f32))
-        wts[k] = jnp.where(here, jnp.where(r0 == expert, w0, w1), 0.0)
-    wtg[0] = wts[0]
+    place = jnp.bitwise_and(lane, 15)
+    plane = jnp.bitwise_xor(z, jnp.bitwise_and(lax.shift_right_logical(lane, 4), 3))
+    expert = (2 * plane + jnp.where(lane < 64, g, 1 - g)).astype(f32)
+    ahead = lax.broadcasted_iota(jnp.int32, (rows, rows), 1)
+    behind = lax.broadcasted_iota(jnp.int32, (rows, rows), 0)
+    before = (ahead < behind).astype(f32).astype(bf16)
+    unit = (ahead == behind).astype(f32)
+    upright = lambda v: lax.dot_general(
+        unit, v, (((1,), (1,)), ((), ())), precision=lax.Precision.HIGHEST, preferred_element_type=f32
+    )
+    named_here, weight_here = upright(routes_ref[...].astype(f32)), upright(rw_ref[...])
+    first, second_one = named_here[:, 0:1] == expert, named_here[:, 1:2] == expert
+    named = first | second_one
+    earlier = dot(before, jnp.where(named, 1.0, 0.0).astype(bf16))
+    here = named & (place < CAP) & (earlier == place.astype(f32))
+    picks[...] = jnp.where(here, 1.0, 0.0).astype(bf16)
+    weights = jnp.where(here, jnp.where(first, weight_here[:, 0:1], weight_here[:, 1:2]), 0.0)
+    high = weights.astype(bf16)
+    w_high[...] = high
+    w_low[...] = (weights - high.astype(f32)).astype(bf16)
 
     pl.semaphore_wait(barrier, len(peers))
     c_part = send(part_ref, other_part, partner)
-    c_wt = {k: send(wts.at[k], wtg.at[k], z_peer[k]) for k in near}
 
     c_part.wait_recv()
     total = tok_ref[...].astype(f32) + (part_ref[...].astype(f32) + other_part[...].astype(f32))
@@ -223,20 +233,16 @@
     expert_in = rms(res_b.astype(f32), gain_ref[...]).astype(bf16)
     xe[0] = expert_in[:, :HALF]
     xe[1] = expert_in[:, HALF:]
-    xg[0] = xe[t]
-    c_x = {k: send(xg.at[0], xg.at[k], z_peer[k]) for k in near}
-    for k in near:
-        c_wt[k].wait_recv()
-    for k in near:
-        c_x[k].wait_recv()
-
-    weights = wtg[...].reshape(4 * rows, LANES)
-    picks = jnp.where(weights > 0.0, 1.0, 0.0).astype(bf16)
-    packed = lax.dot_general(
-        picks, xg[...].reshape(4 * rows, HALF), (((0,), (0,)), ((), ())), preferred_element_type=f32
-    ).astype(bf16)
-    xf[t, 0, 0] = packed[0:BLOCK]
-    cross_out[...] = packed[64 : 64 + BLOCK]
+    pk[...] = lax.dot_general(
+        picks[...], xe[t], (((0,), (0,)), ((), ())), preferred_element_type=f32
+    ).astype(bf16).reshape(8, 16, HALF)
+    sb[0, 0] = pk[0]
+    c_s0 = {k: send(pk.at[k], sb.at[0, k], z_peer[k]) for k in near}
+    c_s1 = {k: send(pk.at[4 + k], sb.at[1, k], z_cross[k]) for k in (0, 1, 3, 2)}
+    r_i = lax.broadcasted_iota(jnp.int32, (BLOCK, 64), 0)
+    c_i = lax.broadcasted_iota(jnp.int32, (BLOCK, 64), 1)
+    r_k = lax.shift_right_logical(r_i * 43, 9)
+    tight = (c_i == 16 * r_k + (r_i - CAP * r_k)).astype(f32).astype(bf16)
 
     mine_at = lambda d, q: xf.at[t, d, q]
     fwd = {}
@@ -244,27 +250,32 @@
     def forward(d, q):
         fwd[d, q] = send(mine_at(d, q), mine_at(d, q), partner)
 
-    c_cross = send(cross_out, mine_at(0, 2), y_cross)
-    c_ax = {d: send(mine_at(0, 0), mine_at(d, 0), x_peer[d]) for d in near}
+    for k in near:
+        c_s0[k].wait_recv()
+    xf[t, 0, 0] = dot(tight, sb[0].reshape(64, HALF)).astype(bf16)
+    c_ax = {d: send(mine_at(0, 0), mine_at(d, 0), x_peer[d]) for d in AX_ORDER}
     c_ay = {0: send(mine_at(0, 0), mine_at(0, 1), y_peer)}
     forward(0, 0)
-    c_cross.wait_recv()
+    for k in (0, 1, 3, 2):
+        c_s1[k].wait_recv()
+    xf[t, 0, 2] = dot(tight, sb[1].reshape(64, HALF)).astype(bf16)
     c_by = send(mine_at(0, 2), mine_at(0, 3), y_peer)
-    c_bx = {(d, 2): send(mine_at(0, 2), mine_at(d, 2), x_peer[d]) for d in near}
+    c_bx = {(d, 2): send(mine_at(0, 2), mine_at(d, 2), x_peer[d]) for d in AX_ORDER}
     forward(0, 2)
-    for d in (1, 3):
+    for d in AX_ORDER[:2]:
         c_ax[d].wait_recv()
         c_ay[d] = send(mine_at(d, 0), mine_at(d, 1), y_peer)
         forward(d, 0)
     c_ay[0].wait_recv()
     forward(0, 1)
     c_by.wait_recv()
-    for d in near:
+    for d in AX_ORDER:
         c_bx[d, 3] = send(mine_at(0, 3), mine_at(d, 3), x_peer[d])
     forward(0, 3)
-    c_ax[2].wait_recv()
-    c_ay[2] = send(mine_at(2, 0), mine_at(2, 1), y_peer)
-    forward(2, 0)
+    d = AX_ORDER[2]
+    c_ax[d].wait_recv()
+    c_ay[d] = send(mine_at(d, 0), mine_at(d, 1), y_peer)
+    forward(d, 0)
 
     for c in loads:
         c.wait()
@@ -325,25 +336,24 @@
     crossed = ys[0, 2:4].astype(f32) + rxc[1].astype(f32) + rxc[3].astype(f32) + rxc[2].astype(f32)
     c_out[...] = crossed[1].astype(bf16)
     c_rc = send(c_out, rc, y_peer)
+    spread = lambda v: lax.dot_general(
+        tight, v.astype(bf16), (((0,), (0,)), ((), ())), preferred_element_type=f32
+    ).astype(bf16).reshape(4, 16, HALF)
     for d in near:
         c_xo[d].wait_recv()
     own = zs_out[0].astype(f32) + rxo[1].astype(f32) + rxo[3].astype(f32) + rxo[2].astype(f32)
-    rb[...] = jnp.zeros(rb.shape, bf16)
-    rb[0:BLOCK] = own.astype(bf16)
+    er[0] = spread(own)
+    rb[0, 0] = er[0, 0]
+    c_r0 = {k: send(er.at[0, k], rb.at[0, k], z_peer[k]) for k in near}
     c_rc.wait_recv()
-    cf_out[...] = (crossed[0] + rc[...].astype(f32)).astype(bf16)
-    c_rr = send(cf_out, rr, y_cross)
-    high = weights.astype(bf16)
-    low = (weights - high.astype(f32)).astype(bf16)
-    c_rr.wait_recv()
-    rb[64 : 64 + BLOCK] = rr[...]
-    back = dot(high, rb[...]) + dot(low, rb[...])
-    u_out[...] = back.astype(bf16).reshape(4, rows, HALF)
-    c_u = {k: send(u_out.at[k], ur.at[k], z_peer[k]) for k in near}
-    mixture = res[t].astype(f32) + back[0:rows]
+    er[1] = spread(crossed[0] + rc[...].astype(f32))
+    c_r1 = {k: send(er.at[1, k], rb.at[1, k], z_cross[k]) for k in (2, 1, 3, 0)}
     for k in near:
-        c_u[k].wait_recv()
-    mixture = mixture + ur[1].astype(f32) + ur[2].astype(f32) + ur[3].astype(f32)
+        c_r0[k].wait_recv()
+    for k in (2, 1, 3, 0):
+        c_r1[k].wait_recv()
+    returned = rb[...].reshape(LANES, HALF)
+    mixture = res[t].astype(f32) + dot(w_high[...], returned) + dot(w_low[...], returned)
     fo[t] = mixture.astype(bf16)
     c_fo = send(fo.at[t], fo.at[t], partner)
     c_fo.wait_recv()
@@ -371,10 +381,11 @@
             pltpu.VMEM((rows, width), bf16),
             pltpu.VMEM((2, rows, HALF), bf16),
             pltpu.VMEM((2, rows, HALF), bf16),
-            pltpu.VMEM((4, rows, LANES), f32),
-            pltpu.VMEM((4, rows, LANES), f32),
-            pltpu.VMEM((4, rows, HALF), bf16),
-            blocks(),
+            pltpu.VMEM((rows, LANES), bf16),
+            pltpu.VMEM((rows, LANES), bf16),
+            pltpu.VMEM((rows, LANES), bf16),
+            pltpu.VMEM((8, 16, HALF), bf16),
+            pltpu.VMEM((2, 4, 16, HALF), bf16),
             blocks(2, 4, 4),
             pltpu.VMEM((4, CHUNK, HALF), f32),
             pltpu.VMEM((4, CHUNK, HALF), bf16),
@@ -386,11 +397,8 @@
             blocks(4, 2),
             blocks(),
             blocks(),
-            blocks(),
-            blocks(),
-            pltpu.VMEM((LANES, HALF), bf16),
-            pltpu.VMEM((4, rows, HALF), bf16),
-            pltpu.VMEM((4, rows, HALF), bf16),
+            pltpu.VMEM((2, 4, 16, HALF), bf16),
+            pltpu.VMEM((2, 4, 16, HALF), bf16),
             pltpu.VMEM((2, rows, HALF), bf16),
             pltpu.SemaphoreType.DMA((4,)),
             pltpu.SemaphoreType.DMA((64,)),
@@ -401,7 +409,7 @@
         ),
         cost_estimate=pl.CostEstimate(flops=5_000_000_000, bytes_accessed=8_000_000, transcendentals=400_000),
         name="routed_experts",
-    )(partial_out, tokens, gain.reshape(1, width), routes, route_weights, wg, wu, wd)
+    )(partial_out, tokens, gain.reshape(1, width), routes.T, route_weights.T, wg, wu, wd)
 
 
 def on_device(

time: 94.5 us -> 82.2 us (0.87)
  Pallas kernels: 89.6 us -> 80.2 us
  local copies, waits for them, and re-layouts: 4.7 us -> 1.57 us
    pallas_call x1, Pallas kernels: 22.6 us -> 17.7 us  [attention(): pl.pallas_call(attention_kernel, out_shape=jax.ShapeDtypeStruct((SEQS, wi...]
    pallas_call x1, Pallas kernels: 67 us -> 62.5 us  [moe(): pl.pallas_call(moe_kernel, out_shape=jax.ShapeDtypeStruct((rows, width),...]
    unnamed x8 -> x1, local copies, waits for them, and re-layouts: 4.7 us -> 1.57 us
where the time goes in v3:
time: 82.2 us; the launch traced here: 81.8 us
  Pallas kernels  80.2 us (98%)
  local copies, waits for them, and re-layouts  1.57 us (2%)
    pallas_call x1, Pallas kernels, moe(): pl.pallas_call(moe_kernel, out_shape=jax.ShapeDtypeStruct((rows, width),...  62.5 us
    pallas_call x1, Pallas kernels, attention(): pl.pallas_call(attention_kernel, out_shape=jax.ShapeDtypeStruct((SEQS, wi...  17.7 us

profile of v3, /device:TPU:1, one launch (start us, length us, event | category | flops | bytes accessed | tf_op | source)
XLA Modules:
  0.0 81.8 jit_solution(920429917569986961)
XLA Ops:
  0.0 17.7 %attention.1.part_ref = bf16[32,2048]{1,0:T(8,128)(2,1)} custom-call(s32[32]{0:T(128)} %len_ref.1, bf16[32,2048]{1,0:T(8,128)(2,1)} %tok_ref.1, bf16[32,1024,128]{2,1,0:T(8,128)(2,1)} %key_hbm.1, bf16[32,1024,128]{2,1,0:T(8,128)(2,1)} %value_hbm.1, f32[32,8,1024]{2,1,0:T(8,128)} %gate_hbm.1, f32[1,2048]{1,0:T(1,128)} %bitcast.6, bf16[2048,512]{1,0:T(8,128)(2,1)} %wq_hbm.1, ...), custom_call_target="tpu_custom_call" | custom-call | flops 500000000 | bytes 24000000 | tf_op jit(solution)/shard_map/attention/pallas_call | solution.py:114
  17.7 62.5 %routed_experts.1 = bf16[32,2048]{1,0:T(8,128)(2,1)} custom-call(bf16[32,2048]{1,0:T(8,128)(2,1)} %attention.1.part_ref, bf16[32,2048]{1,0:T(8,128)(2,1)} %tok_ref.1, f32[1,2048]{1,0:T(1,128)} %bitcast.7, s32[2,32]{1,0:T(2,128)} %bitcast.8, f32[2,32]{1,0:T(2,128)} %bitcast.9, bf16[2048,512]{1,0:T(8,128)(2,1)} %wg_hbm.1, bf16[2048,512]{1,0:T(8,128)(2,1)} %wu_hbm.1, ...), custom_call_target="tpu_custom_call" | custom-call | flops 5000000000 | bytes 8000000 | tf_op jit(solution)/shard_map/routed_experts/pallas_call | solution.py:372
  80.2 1.6 %copy.19 = bf16[32,2048]{1,0:T(8,128)(2,1)} copy(bf16[32,2048]{1,0:T(8,128)(2,1)} %routed_experts.1) | data formatting | bytes 262144

commit v4 on v3

--- a/solution.py
+++ b/solution.py
@@ -72,24 +72,31 @@
         with jax.named_scope("wait_kv"):
             for c in block_copies(b):
                 c.wait()
-        for j in range(per):
-            s = b * per + j
-            rows = pl.ds(s * HEADS_HERE, HEADS_HERE)
+        seqs = [b * per + j for j in range(per)]
+        rows = [pl.ds(s * HEADS_HERE, HEADS_HERE) for s in seqs]
+        scores = [
+            lax.dot_general(
+                qs[r, :].astype(jnp.bfloat16), keys[s], (((1,), (1,)), ((), ())),
+                preferred_element_type=jnp.float32,
+            )
+            for s, r in zip(seqs, rows)
+        ]
+        raised, scale, own_part = [], [], []
+        for s, r, score in zip(seqs, rows, scores):
             length = len_ref[s]
             g = gates[s]
-            score = lax.dot_general(
-                qs[rows, :].astype(jnp.bfloat16), keys[s], (((1,), (1,)), ((), ())),
-                preferred_element_type=jnp.float32,
-            )
             latest = jnp.sum(jnp.where(position == length - 1, g, 0.0), axis=1, keepdims=True)
-            own = owns[rows, 0:1]
-            score = jnp.where(position < length, score + (latest + lgs[rows, 0:1]) - g, -jnp.inf)
+            own = owns[r, 0:1]
+            score = jnp.where(position < length, score + (latest + lgs[r, 0:1]) - g, -jnp.inf)
             top = jnp.maximum(jnp.max(score, axis=1, keepdims=True), own)
-            raised = jnp.exp(score - top)
+            lifted = jnp.exp(score - top)
             own_raised = jnp.exp(own - top)
-            total = jnp.sum(raised, axis=1, keepdims=True) + own_raised
-            o = dot(raised.astype(jnp.bfloat16), values[s])
-            mixed[rows, :] = (o + own_raised * vnew[pl.ds(s, 1), :]) / total
+            raised.append(lifted.astype(jnp.bfloat16))
+            scale.append(1.0 / (jnp.sum(lifted, axis=1, keepdims=True) + own_raised))
+            own_part.append(own_raised * vnew[pl.ds(s, 1), :])
+        sums = [dot(p, values[s]) for p, s in zip(raised, seqs)]
+        for r, o, c, w in zip(rows, sums, scale, own_part):
+            mixed[r, :] = (o + w) * c
         return carry
 
     with jax.named_scope("loop"):
@@ -106,7 +113,7 @@
     out_ref[...] = dot(jnp.concatenate(parts, axis=1), wo[...]).astype(jnp.bfloat16)
 
 
-def attention(tokens, lengths, key_cache, value_cache, gate_cache, gain, wq, wk, wv, wf, wo, blocks=8):
+def attention(tokens, lengths, key_cache, value_cache, gate_cache, gain, wq, wk, wv, wf, wo, blocks=4):
     wf = wf.T
     width = tokens.shape[1]
     f32, bf16 = jnp.float32, jnp.bfloat16
@@ -146,7 +153,7 @@
 HALF = 1024
 BLOCK = 48
 CHUNK = 4 * BLOCK
-AX_ORDER = (1, 3, 2)
+AX_ORDER = (2, 1, 3)
 
 
 def moe_kernel(
@@ -316,20 +323,20 @@
             c_xo[d] = send(zs_out.at[d], rxo.at[d], x_peer[d])
 
     compute(0)
+    arrive(2)
     arrive(1)
-    compute(1)
+    compute(2)
     finish(0)
     arrive(3)
+    compute(1)
+    finish(2)
     compute(3)
+    second(2)
     finish(1)
-    second(0)
-    arrive(2)
-    compute(2)
     finish(3)
     second(1)
-    finish(2)
     second(3)
-    second(2)
+    second(0)
 
     for d in near:
         c_xc[d].wait_recv()

time: 82.2 us -> 70.8 us (0.86)
  Pallas kernels: 80.2 us -> 69.1 us
    pallas_call x1, Pallas kernels: 17.7 us -> 10.3 us  [attention(): pl.pallas_call(attention_kernel, out_shape=jax.ShapeDtypeStruct((SEQS, wi...]
    pallas_call x1, Pallas kernels: 62.5 us -> 58.7 us  [moe(): pl.pallas_call(moe_kernel, out_shape=jax.ShapeDtypeStruct((rows, width),...]
where the time goes in v4:
time: 70.8 us; the launch traced here: 70.6 us
  Pallas kernels  69.1 us (98%)
  local copies, waits for them, and re-layouts  1.57 us (2%)
    pallas_call x1, Pallas kernels, moe(): pl.pallas_call(moe_kernel, out_shape=jax.ShapeDtypeStruct((rows, width),...  58.7 us
    pallas_call x1, Pallas kernels, attention(): pl.pallas_call(attention_kernel, out_shape=jax.ShapeDtypeStruct((SEQS, wi...  10.3 us
    unnamed x1, local copies, waits for them, and re-layouts  1.57 us

profile of v4, /device:TPU:1, one launch (start us, length us, event | category | flops | bytes accessed | tf_op | source)
XLA Modules:
  0.0 70.6 jit_solution(16527002457149889326)
XLA Ops:
  0.0 10.3 %attention.1.part_ref = bf16[32,2048]{1,0:T(8,128)(2,1)} custom-call(s32[32]{0:T(128)} %len_ref.1, bf16[32,2048]{1,0:T(8,128)(2,1)} %tok_ref.1, bf16[32,1024,128]{2,1,0:T(8,128)(2,1)} %key_hbm.1, bf16[32,1024,128]{2,1,0:T(8,128)(2,1)} %value_hbm.1, f32[32,8,1024]{2,1,0:T(8,128)} %gate_hbm.1, f32[1,2048]{1,0:T(1,128)} %bitcast.6, bf16[2048,512]{1,0:T(8,128)(2,1)} %wq_hbm.1, ...), custom_call_target="tpu_custom_call" | custom-call | flops 500000000 | bytes 24000000 | tf_op jit(solution)/shard_map/attention/pallas_call | solution.py:121
  10.3 58.7 %routed_experts.1 = bf16[32,2048]{1,0:T(8,128)(2,1)} custom-call(bf16[32,2048]{1,0:T(8,128)(2,1)} %attention.1.part_ref, bf16[32,2048]{1,0:T(8,128)(2,1)} %tok_ref.1, f32[1,2048]{1,0:T(1,128)} %bitcast.7, s32[2,32]{1,0:T(2,128)} %bitcast.8, f32[2,32]{1,0:T(2,128)} %bitcast.9, bf16[2048,512]{1,0:T(8,128)(2,1)} %wg_hbm.1, bf16[2048,512]{1,0:T(8,128)(2,1)} %wu_hbm.1, ...), custom_call_target="tpu_custom_call" | custom-call | flops 5000000000 | bytes 8000000 | tf_op jit(solution)/shard_map/routed_experts/pallas_call | solution.py:379
  69.1 1.6 %copy.19 = bf16[32,2048]{1,0:T(8,128)(2,1)} copy(bf16[32,2048]{1,0:T(8,128)(2,1)} %routed_experts.1) | data formatting | bytes 262144

commit v5 on v4

--- a/solution.py
+++ b/solution.py
@@ -10,14 +10,15 @@
 POS = 1024
 LANES = 128
 HEADS_HERE = 8
+KV_BLOCKS = 4
 
 
 def rms(values, gain):
     return values * lax.rsqrt(jnp.mean(values * values, axis=-1, keepdims=True) + 1e-06) * gain
 
 
-def attention_kernel(
-    len_ref, tok_hbm, key_hbm, value_hbm, gate_hbm, gain_hbm, wq_hbm, wk_hbm, wv_hbm, wf_hbm, wo_hbm,
+def attend(
+    then, meanwhile, len_ref, tok_hbm, key_hbm, value_hbm, gate_hbm, gain_hbm, wq_hbm, wk_hbm, wv_hbm, wf_hbm, wo_hbm,
     out_ref,
     tok, gain, wq, wk, wv, wf, wo, keys, values, gates, qs, owns, lgs, vnew, mixed, sems, kv_sems,
 ):
@@ -34,6 +35,7 @@
 
     for c in copies[:6]:
         c.start()
+    meanwhile()
     with jax.named_scope("wait_tok"):
         copies[0].wait()
         copies[1].wait()
@@ -50,6 +52,7 @@
         for c in block_copies(b):
             c.start()
     copies[6].start()
+    then()
     dot = functools.partial(jnp.dot, preferred_element_type=jnp.float32)
     q = dot(ni, wq[...]).astype(jnp.bfloat16).astype(jnp.float32) * 0.125
     kn = dot(ni, wk[...]).astype(jnp.bfloat16).astype(jnp.float32)
@@ -113,56 +116,28 @@
     out_ref[...] = dot(jnp.concatenate(parts, axis=1), wo[...]).astype(jnp.bfloat16)
 
 
-def attention(tokens, lengths, key_cache, value_cache, gate_cache, gain, wq, wk, wv, wf, wo, blocks=4):
-    wf = wf.T
-    width = tokens.shape[1]
-    f32, bf16 = jnp.float32, jnp.bfloat16
-    any_space = pl.BlockSpec(memory_space=pl.ANY)
-    return pl.pallas_call(
-        attention_kernel,
-        out_shape=jax.ShapeDtypeStruct((SEQS, width), bf16),
-        in_specs=[pl.BlockSpec(memory_space=pltpu.SMEM)] + [any_space] * 10,
-        out_specs=pl.BlockSpec(memory_space=pltpu.VMEM),
-        scratch_shapes=[
-            pltpu.VMEM((SEQS, width), bf16),
-            pltpu.VMEM((1, width), f32),
-            pltpu.VMEM(wq.shape, bf16),
-            pltpu.VMEM(wk.shape, bf16),
-            pltpu.VMEM(wv.shape, bf16),
-            pltpu.VMEM(wf.shape, bf16),
-            pltpu.VMEM(wo.shape, bf16),
-            pltpu.VMEM(key_cache.shape, bf16),
-            pltpu.VMEM(value_cache.shape, bf16),
-            pltpu.VMEM(gate_cache.shape, f32),
-            pltpu.VMEM((SEQS * HEADS_HERE, LANES), f32),
-            pltpu.VMEM((SEQS * HEADS_HERE, LANES), f32),
-            pltpu.VMEM((SEQS * HEADS_HERE, LANES), f32),
-            pltpu.VMEM((SEQS, LANES), f32),
-            pltpu.VMEM((SEQS * HEADS_HERE, LANES), f32),
-            pltpu.SemaphoreType.DMA((7,)),
-            pltpu.SemaphoreType.DMA((3, blocks)),
-        ],
-        compiler_params=pltpu.CompilerParams(vmem_limit_bytes=60 * 1024 * 1024),
-        cost_estimate=pl.CostEstimate(flops=500_000_000, bytes_accessed=24_000_000, transcendentals=300_000),
-        name="attention",
-    )(lengths, tokens, key_cache, value_cache, gate_cache, gain.reshape(1, width), wq, wk, wv, wf, wo)
-
-
 MESH = pl.DeviceIdType.MESH
 CAP = 12
 HALF = 1024
 BLOCK = 48
 CHUNK = 4 * BLOCK
-AX_ORDER = (2, 1, 3)
-
-
-def moe_kernel(
-    part_ref, tok_ref, gain_ref, routes_ref, rw_ref, wg_hbm, wu_hbm, wd_hbm,
+
+
+ATTEND_SCRATCH = 17
+
+
+def layer_kernel(
+    len_ref, tok_hbm, key_hbm, value_hbm, gate_hbm, mix_hbm, wq_hbm, wk_hbm, wv_hbm, wf_hbm, wo_hbm,
+    gain_hbm, routes_ref, rw_ref, wg_hbm, wu_hbm, wd_hbm,
     out_ref,
-    wg, wu, wd, other_part, res, xe, picks, w_high, w_low, pk, sb, xf,
-    pm, po, pi, ys, ry, zs_out, rxo, rxc, c_out, rc, er, rb, fo,
-    wsem, ss, rs,
+    part_ref, *scratch,
 ):
+    (
+        gain, wg, wu, wd, other_part, res, xe, picks, w_high, w_low, pk, sb, xf,
+        pm, po, pi, ys, ry, zs_out, rxo, rxc, c_out, rc, er, rb, fo, hid, hop_c, hop_o,
+        wsem, ss, rs,
+    ) = scratch[ATTEND_SCRATCH:]
+    tok_ref = scratch[0]
     f32, bf16 = jnp.float32, jnp.bfloat16
     dot = functools.partial(jnp.dot, preferred_element_type=f32)
     e, t = lax.axis_index("ep"), lax.axis_index("tp")
@@ -184,9 +159,8 @@
         pltpu.make_async_copy(wu_hbm, wu, wsem.at[1]),
         pltpu.make_async_copy(wd_hbm.at[:, pl.ds(0, HALF)], wd.at[0], wsem.at[2]),
         pltpu.make_async_copy(wd_hbm.at[:, pl.ds(HALF, HALF)], wd.at[1], wsem.at[3]),
+        pltpu.make_async_copy(gain_hbm, gain, wsem.at[4]),
     ]
-    for c in loads:
-        c.start()
 
     count = [0]
     started = []
@@ -207,28 +181,39 @@
         pl.semaphore_signal(barrier, inc=1, device_id=p, device_id_type=MESH)
 
     rows = tok_ref.shape[0]
-    lane = lax.broadcasted_iota(jnp.int32, (rows, LANES), 1)
-    place = jnp.bitwise_and(lane, 15)
-    plane = jnp.bitwise_xor(z, jnp.bitwise_and(lax.shift_right_logical(lane, 4), 3))
-    expert = (2 * plane + jnp.where(lane < 64, g, 1 - g)).astype(f32)
-    ahead = lax.broadcasted_iota(jnp.int32, (rows, rows), 1)
-    behind = lax.broadcasted_iota(jnp.int32, (rows, rows), 0)
-    before = (ahead < behind).astype(f32).astype(bf16)
-    unit = (ahead == behind).astype(f32)
-    upright = lambda v: lax.dot_general(
-        unit, v, (((1,), (1,)), ((), ())), precision=lax.Precision.HIGHEST, preferred_element_type=f32
+
+    def choose():
+        lane = lax.broadcasted_iota(jnp.int32, (rows, LANES), 1)
+        place = jnp.bitwise_and(lane, 15)
+        plane = jnp.bitwise_xor(z, jnp.bitwise_and(lax.shift_right_logical(lane, 4), 3))
+        expert = (2 * plane + jnp.where(lane < 64, g, 1 - g)).astype(f32)
+        ahead = lax.broadcasted_iota(jnp.int32, (rows, rows), 1)
+        behind = lax.broadcasted_iota(jnp.int32, (rows, rows), 0)
+        before = (ahead < behind).astype(f32).astype(bf16)
+        unit = (ahead == behind).astype(f32)
+        upright = lambda v: lax.dot_general(
+            unit, v, (((1,), (1,)), ((), ())), precision=lax.Precision.HIGHEST, preferred_element_type=f32
+        )
+        named_here, weight_here = upright(routes_ref[...].astype(f32)), upright(rw_ref[...])
+        first, second_one = named_here[:, 0:1] == expert, named_here[:, 1:2] == expert
+        named = first | second_one
+        earlier = dot(before, jnp.where(named, 1.0, 0.0).astype(bf16))
+        here = named & (place < CAP) & (earlier == place.astype(f32))
+        picks[...] = jnp.where(here, 1.0, 0.0).astype(bf16)
+        weights = jnp.where(here, jnp.where(first, weight_here[:, 0:1], weight_here[:, 1:2]), 0.0)
+        high = weights.astype(bf16)
+        w_high[...] = high
+        w_low[...] = (weights - high.astype(f32)).astype(bf16)
+
+    def load():
+        for c in loads:
+            c.start()
+
+    attend(
+        load, choose, len_ref, tok_hbm, key_hbm, value_hbm, gate_hbm, mix_hbm, wq_hbm, wk_hbm, wv_hbm, wf_hbm, wo_hbm,
+        part_ref, *scratch[:ATTEND_SCRATCH],
     )
-    named_here, weight_here = upright(routes_ref[...].astype(f32)), upright(rw_ref[...])
-    first, second_one = named_here[:, 0:1] == expert, named_here[:, 1:2] == expert
-    named = first | second_one
-    earlier = dot(before, jnp.where(named, 1.0, 0.0).astype(bf16))
-    here = named & (place < CAP) & (earlier == place.astype(f32))
-    picks[...] = jnp.where(here, 1.0, 0.0).astype(bf16)
-    weights = jnp.where(here, jnp.where(first, weight_here[:, 0:1], weight_here[:, 1:2]), 0.0)
-    high = weights.astype(bf16)
-    w_high[...] = high
-    w_low[...] = (weights - high.astype(f32)).astype(bf16)
-
+    loads[4].wait()
     pl.semaphore_wait(barrier, len(peers))
     c_part = send(part_ref, other_part, partner)
 
@@ -237,7 +222,7 @@
     res_b = total.astype(bf16)
     res[0] = res_b[:, :HALF]
     res[1] = res_b[:, HALF:]
-    expert_in = rms(res_b.astype(f32), gain_ref[...]).astype(bf16)
+    expert_in = rms(res_b.astype(f32), gain[...]).astype(bf16)
     xe[0] = expert_in[:, :HALF]
     xe[1] = expert_in[:, HALF:]
     pk[...] = lax.dot_general(
@@ -260,44 +245,62 @@
     for k in near:
         c_s0[k].wait_recv()
     xf[t, 0, 0] = dot(tight, sb[0].reshape(64, HALF)).astype(bf16)
-    c_ax = {d: send(mine_at(0, 0), mine_at(d, 0), x_peer[d]) for d in AX_ORDER}
-    c_ay = {0: send(mine_at(0, 0), mine_at(0, 1), y_peer)}
-    forward(0, 0)
+    c_ax, c_ay, c_bx = {}, {}, {}
+
+    def ax(d):
+        c_ax[d] = send(mine_at(0, 0), mine_at(d, 0), x_peer[d])
+
+    def bx(d, q):
+        c_bx[d, q] = send(mine_at(0, q), mine_at(d, q), x_peer[d])
+
+    def ay(d):
+        if d:
+            c_ax[d].wait_recv()
+        c_ay[d] = send(mine_at(d, 0), mine_at(d, 1), y_peer)
+        forward(d, 0)
+
+    ax(2)
+    ay(0)
     for k in (0, 1, 3, 2):
         c_s1[k].wait_recv()
     xf[t, 0, 2] = dot(tight, sb[1].reshape(64, HALF)).astype(bf16)
     c_by = send(mine_at(0, 2), mine_at(0, 3), y_peer)
-    c_bx = {(d, 2): send(mine_at(0, 2), mine_at(d, 2), x_peer[d]) for d in AX_ORDER}
+    bx(2, 2)
+    ax(1)
+    ax(3)
     forward(0, 2)
-    for d in AX_ORDER[:2]:
-        c_ax[d].wait_recv()
-        c_ay[d] = send(mine_at(d, 0), mine_at(d, 1), y_peer)
-        forward(d, 0)
+    ay(2)
     c_ay[0].wait_recv()
     forward(0, 1)
     c_by.wait_recv()
-    for d in AX_ORDER:
-        c_bx[d, 3] = send(mine_at(0, 3), mine_at(d, 3), x_peer[d])
+    bx(2, 3)
     forward(0, 3)
-    d = AX_ORDER[2]
-    c_ax[d].wait_recv()
-    c_ay[d] = send(mine_at(d, 0), mine_at(d, 1), y_peer)
-    forward(d, 0)
-
-    for c in loads:
+    bx(1, 2)
+    bx(3, 2)
+    bx(1, 3)
+    bx(3, 3)
+    ay(1)
+    ay(3)
+    for c in loads[:4]:
         c.wait()
     c_pi = {}
 
-    def compute(d):
+    def hide(d):
         for q in range(4):
             fwd[d, q].wait_recv()
         x0, x1 = xf[0, d].reshape(CHUNK, HALF), xf[1, d].reshape(CHUNK, HALF)
         gate = dot(x0, wg[0:HALF]) + dot(x1, wg[HALF : 2 * HALF])
         up = dot(x0, wu[0:HALF]) + dot(x1, wu[HALF : 2 * HALF])
-        hidden = (gate / (1.0 + jnp.exp(-gate)) * up).astype(bf16)
-        po[d] = dot(hidden, wd[1 - t]).astype(bf16)
+        hid[d] = (gate / (1.0 + jnp.exp(-gate)) * up).astype(bf16)
+
+    def down(d):
+        po[d] = dot(hid[d], wd[1 - t]).astype(bf16)
         c_pi[d] = send(po.at[d], pi.at[d], partner)
-        pm[d] = dot(hidden, wd[t])
+        pm[d] = dot(hid[d], wd[t])
+
+    def compute(d):
+        hide(d)
+        down(d)
 
     c_ry, c_xc, c_xo = {}, {}, {}
 
@@ -309,46 +312,63 @@
         c_bx[d, 3].wait_recv()
         forward(d, 3)
 
+    side = {1: pl.ds(HALF // 2, HALF // 2), 3: pl.ds(0, HALF // 2)}
+
     def finish(d):
         c_pi[d].wait_recv()
         ys[d] = (pm[d] + pi[d].astype(f32)).astype(bf16).reshape(4, BLOCK, HALF)
-        if d:
-            c_xc[d] = send(ys.at[d, pl.ds(2, 2)], rxc.at[d], x_peer[d])
         c_ry[d] = send(ys.at[d, 1], ry.at[d], y_peer)
+        if d == 2:
+            for n in (1, 3):
+                c_xc[2, n] = send(ys.at[2, pl.ds(2, 2), :, side[4 - n]], hop_c.at[n], x_peer[n])
+
+    def across(d):
+        c_xc[2, 4 - d].wait_recv()
+        ys[d, 2:4, :, side[d]] = (ys[d, 2:4, :, side[d]].astype(f32) + hop_c[4 - d].astype(f32)).astype(bf16)
+        c_xc[d] = send(ys.at[d, pl.ds(2, 2)], rxc.at[d], x_peer[d])
 
     def second(d):
         c_ry[d].wait_recv()
         zs_out[d] = (ys[d, 0].astype(f32) + ry[d].astype(f32)).astype(bf16)
-        if d:
+        if d == 2:
+            for n in (1, 3):
+                c_xo[2, n] = send(zs_out.at[2, :, side[4 - n]], hop_o.at[n], x_peer[n])
+        elif d:
+            c_xo[2, 4 - d].wait_recv()
+            zs_out[d, :, side[d]] = (zs_out[d, :, side[d]].astype(f32) + hop_o[4 - d].astype(f32)).astype(bf16)
             c_xo[d] = send(zs_out.at[d], rxo.at[d], x_peer[d])
 
     compute(0)
     arrive(2)
-    arrive(1)
     compute(2)
     finish(0)
+    arrive(1)
+    hide(1)
+    finish(2)
+    down(1)
     arrive(3)
-    compute(1)
-    finish(2)
     compute(3)
     second(2)
     finish(1)
+    across(1)
     finish(3)
+    across(3)
     second(1)
     second(3)
     second(0)
 
-    for d in near:
+
+    for d in (1, 3):
         c_xc[d].wait_recv()
-    crossed = ys[0, 2:4].astype(f32) + rxc[1].astype(f32) + rxc[3].astype(f32) + rxc[2].astype(f32)
+    crossed = ys[0, 2:4].astype(f32) + rxc[1].astype(f32) + rxc[3].astype(f32)
     c_out[...] = crossed[1].astype(bf16)
     c_rc = send(c_out, rc, y_peer)
     spread = lambda v: lax.dot_general(
         tight, v.astype(bf16), (((0,), (0,)), ((), ())), preferred_element_type=f32
     ).astype(bf16).reshape(4, 16, HALF)
-    for d in near:
+    for d in (1, 3):
         c_xo[d].wait_recv()
-    own = zs_out[0].astype(f32) + rxo[1].astype(f32) + rxo[3].astype(f32) + rxo[2].astype(f32)
+    own = zs_out[0].astype(f32) + rxo[1].astype(f32) + rxo[3].astype(f32)
     er[0] = spread(own)
     rb[0, 0] = er[0, 0]
     c_r0 = {k: send(er.at[0, k], rb.at[0, k], z_peer[k]) for k in near}
@@ -370,21 +390,46 @@
         c.wait_send()
 
 
-def moe(partial_out, tokens, gain, routes, route_weights, wg, wu, wd):
+def on_device(
+    tokens, lengths, key_cache, value_cache, gate_cache, mix_gain, query_weight, key_weight, value_weight,
+    forget_weight, out_weight, expert_gain, routes, route_weights, expert_gate, expert_up, expert_down,
+):
     rows, width = tokens.shape
     f32, bf16 = jnp.float32, jnp.bfloat16
     any_space = pl.BlockSpec(memory_space=pl.ANY)
     vmem = pl.BlockSpec(memory_space=pltpu.VMEM)
+    smem = pl.BlockSpec(memory_space=pltpu.SMEM)
     blocks = lambda *s: pltpu.VMEM((*s, BLOCK, HALF), bf16)
+    heads = pltpu.VMEM((SEQS * HEADS_HERE, LANES), f32)
+    forget = forget_weight.T
     return pl.pallas_call(
-        moe_kernel,
+        layer_kernel,
         out_shape=jax.ShapeDtypeStruct((rows, width), bf16),
-        in_specs=[vmem] * 5 + [any_space] * 3,
+        in_specs=[smem] + [any_space] * 11 + [vmem] * 2 + [any_space] * 3,
         out_specs=vmem,
         scratch_shapes=[
-            pltpu.VMEM(wg.shape, bf16),
-            pltpu.VMEM(wu.shape, bf16),
-            pltpu.VMEM((2, wd.shape[0], HALF), bf16),
+            pltpu.VMEM((rows, width), bf16),
+            pltpu.VMEM((rows, width), bf16),
+            pltpu.VMEM((1, width), f32),
+            pltpu.VMEM(query_weight.shape, bf16),
+            pltpu.VMEM(key_weight.shape, bf16),
+            pltpu.VMEM(value_weight.shape, bf16),
+            pltpu.VMEM(forget.shape, bf16),
+            pltpu.VMEM(out_weight.shape, bf16),
+            pltpu.VMEM(key_cache.shape, bf16),
+            pltpu.VMEM(value_cache.shape, bf16),
+            pltpu.VMEM(gate_cache.shape, f32),
+            heads,
+            heads,
+            heads,
+            pltpu.VMEM((SEQS, LANES), f32),
+            heads,
+            pltpu.SemaphoreType.DMA((7,)),
+            pltpu.SemaphoreType.DMA((3, KV_BLOCKS)),
+            pltpu.VMEM((1, width), f32),
+            pltpu.VMEM(expert_gate.shape, bf16),
+            pltpu.VMEM(expert_up.shape, bf16),
+            pltpu.VMEM((2, expert_down.shape[0], HALF), bf16),
             pltpu.VMEM((rows, width), bf16),
             pltpu.VMEM((2, rows, HALF), bf16),
             pltpu.VMEM((2, rows, HALF), bf16),
@@ -407,27 +452,23 @@
             pltpu.VMEM((2, 4, 16, HALF), bf16),
             pltpu.VMEM((2, 4, 16, HALF), bf16),
             pltpu.VMEM((2, rows, HALF), bf16),
-            pltpu.SemaphoreType.DMA((4,)),
-            pltpu.SemaphoreType.DMA((64,)),
-            pltpu.SemaphoreType.DMA((64,)),
+            pltpu.VMEM((4, CHUNK, expert_gate.shape[1]), bf16),
+            pltpu.VMEM((4, 2, BLOCK, HALF // 2), bf16),
+            pltpu.VMEM((4, BLOCK, HALF // 2), bf16),
+            pltpu.SemaphoreType.DMA((5,)),
+            pltpu.SemaphoreType.DMA((72,)),
+            pltpu.SemaphoreType.DMA((72,)),
         ],
         compiler_params=pltpu.CompilerParams(
-            collective_id=0, has_side_effects=True, vmem_limit_bytes=56 * 1024 * 1024
+            collective_id=0, has_side_effects=True, vmem_limit_bytes=60 * 1024 * 1024
         ),
-        cost_estimate=pl.CostEstimate(flops=5_000_000_000, bytes_accessed=8_000_000, transcendentals=400_000),
-        name="routed_experts",
-    )(partial_out, tokens, gain.reshape(1, width), routes.T, route_weights.T, wg, wu, wd)
-
-
-def on_device(
-    tokens, lengths, key_cache, value_cache, gate_cache, mix_gain, query_weight, key_weight, value_weight,
-    forget_weight, out_weight, expert_gain, routes, route_weights, expert_gate, expert_up, expert_down,
-):
-    partial_out = attention(
-        tokens, lengths, key_cache, value_cache, gate_cache, mix_gain,
-        query_weight, key_weight, value_weight, forget_weight, out_weight,
+        cost_estimate=pl.CostEstimate(flops=5_500_000_000, bytes_accessed=30_000_000, transcendentals=700_000),
+        name="decode_layer",
+    )(
+        lengths, tokens, key_cache, value_cache, gate_cache, mix_gain.reshape(1, width), query_weight, key_weight,
+        value_weight, forget, out_weight, expert_gain.reshape(1, width), routes.T, route_weights.T,
+        expert_gate, expert_up, expert_down,
     )
-    return moe(partial_out, tokens, expert_gain, routes, route_weights, expert_gate, expert_up, expert_down)
 
 
 def solution(mesh):

time: 70.8 us -> 67.5 us (0.953)
  Pallas kernels: 69.1 us -> 65.8 us
    pallas_call x2 -> x1, Pallas kernels: 69.1 us -> 65.8 us  [on_device(): pl.pallas_call(layer_kernel, out_shape=jax.ShapeDtypeStruct((rows, width)...]
where the time goes in v5:
time: 67.5 us; the launch traced here: 67.4 us
  Pallas kernels  65.8 us (97%)
  local copies, waits for them, and re-layouts  1.57 us (2%)
    pallas_call x1, Pallas kernels, on_device(): pl.pallas_call(layer_kernel, out_shape=jax.ShapeDtypeStruct((rows, width)...  65.8 us
    unnamed x1, local copies, waits for them, and re-layouts  1.57 us

profile of v5, /device:TPU:1, one launch (start us, length us, event | category | flops | bytes accessed | tf_op | source)
XLA Modules:
  0.0 67.4 jit_solution(1072920425333958541)
XLA Ops:
  0.0 65.8 %decode_layer.1 = bf16[32,2048]{1,0:T(8,128)(2,1)} custom-call(s32[32]{0:T(128)} %len_ref.1, bf16[32,2048]{1,0:T(8,128)(2,1)} %tok_hbm.1, bf16[32,1024,128]{2,1,0:T(8,128)(2,1)} %key_hbm.1, bf16[32,1024,128]{2,1,0:T(8,128)(2,1)} %value_hbm.1, f32[32,8,1024]{2,1,0:T(8,128)} %gate_hbm.1, f32[1,2048]{1,0:T(1,128)} %bitcast.6, bf16[2048,512]{1,0:T(8,128)(2,1)} %wq_hbm.1, ...), custom_call_target="tpu_custom_call" | custom-call | flops 5500000256 | bytes 30000000 | tf_op jit(solution)/shard_map/decode_layer/pallas_call | solution.py:405
  65.8 1.6 %copy.19 = bf16[32,2048]{1,0:T(8,128)(2,1)} copy(bf16[32,2048]{1,0:T(8,128)(2,1)} %decode_layer.1) | data formatting | bytes 262144

commit v6 on v5

--- a/solution.py
+++ b/solution.py
@@ -18,7 +18,7 @@
 
 
 def attend(
-    then, meanwhile, len_ref, tok_hbm, key_hbm, value_hbm, gate_hbm, gain_hbm, wq_hbm, wk_hbm, wv_hbm, wf_hbm, wo_hbm,
+    first, then, meanwhile, len_ref, tok_hbm, key_hbm, value_hbm, gate_hbm, gain_hbm, wq_hbm, wk_hbm, wv_hbm, wf_hbm, wo_hbm,
     out_ref,
     tok, gain, wq, wk, wv, wf, wo, keys, values, gates, qs, owns, lgs, vnew, mixed, sems, kv_sems,
 ):
@@ -33,7 +33,10 @@
             for i, (src, dst) in enumerate(((key_hbm, keys), (gate_hbm, gates), (value_hbm, values)))
         ]
 
-    for c in copies[:6]:
+    copies[0].start()
+    copies[1].start()
+    first()
+    for c in copies[2:6]:
         c.start()
     meanwhile()
     with jax.named_scope("wait_tok"):
@@ -52,7 +55,6 @@
         for c in block_copies(b):
             c.start()
     copies[6].start()
-    then()
     dot = functools.partial(jnp.dot, preferred_element_type=jnp.float32)
     q = dot(ni, wq[...]).astype(jnp.bfloat16).astype(jnp.float32) * 0.125
     kn = dot(ni, wk[...]).astype(jnp.bfloat16).astype(jnp.float32)
@@ -104,6 +106,7 @@
 
     with jax.named_scope("loop"):
         lax.fori_loop(0, blocks, block, 0)
+    then()
     parts = []
     for c in range(4):
         pair = []
@@ -127,14 +130,14 @@
 
 
 def layer_kernel(
-    len_ref, tok_hbm, key_hbm, value_hbm, gate_hbm, mix_hbm, wq_hbm, wk_hbm, wv_hbm, wf_hbm, wo_hbm,
-    gain_hbm, routes_ref, rw_ref, wg_hbm, wu_hbm, wd_hbm,
+    len_hbm, tok_hbm, key_hbm, value_hbm, gate_hbm, mix_hbm, wq_hbm, wk_hbm, wv_hbm, wf_hbm, wo_hbm,
+    gain_hbm, routes_hbm, rw_hbm, wg_hbm, wu_hbm, wd_hbm,
     out_ref,
     part_ref, *scratch,
 ):
     (
-        gain, wg, wu, wd, other_part, res, xe, picks, w_high, w_low, pk, sb, xf,
-        pm, po, pi, ys, ry, zs_out, rxo, rxc, c_out, rc, er, rb, fo, hid, hop_c, hop_o,
+        len_ref, routes_ref, rw_ref, gain, wg, wu, wd, other_part, res, xe, picks, w_high, w_low, pk, sb, xf,
+        pm, po, pi, ys, ry, zs_out, rxo, rxc, er, rb, fo, hid, hop_c, hop_o,
         wsem, ss, rs,
     ) = scratch[ATTEND_SCRATCH:]
     tok_ref = scratch[0]
@@ -152,6 +155,7 @@
     x_peer = {k: chip(z, y, jnp.bitwise_xor(x, k)) for k in (1, 2, 3)}
     y_peer = chip(z, jnp.bitwise_xor(y, 1), x)
     z_cross = {k: chip(jnp.bitwise_xor(z, k), 3 - y, x) for k in range(4)}
+    z_far = {k: chip(jnp.bitwise_xor(z, k), jnp.bitwise_xor(y, 2), x) for k in range(4)}
     near = (1, 3, 2)
 
     loads = [
@@ -161,6 +165,15 @@
         pltpu.make_async_copy(wd_hbm.at[:, pl.ds(HALF, HALF)], wd.at[1], wsem.at[3]),
         pltpu.make_async_copy(gain_hbm, gain, wsem.at[4]),
     ]
+    tables = [
+        pltpu.make_async_copy(routes_hbm, routes_ref, wsem.at[5]),
+        pltpu.make_async_copy(rw_hbm, rw_ref, wsem.at[6]),
+        pltpu.make_async_copy(len_hbm, len_ref, wsem.at[7]),
+    ]
+
+    def first_loads():
+        for c in (*tables, loads[4]):
+            c.start()
 
     count = [0]
     started = []
@@ -176,13 +189,15 @@
         return c
 
     barrier = pltpu.get_barrier_semaphore()
-    peers = [partner, y_peer, *z_peer.values(), *z_cross.values(), *x_peer.values()]
+    peers = [partner, y_peer, *z_peer.values(), *z_cross.values(), *z_far.values(), *x_peer.values()]
     for p in peers:
         pl.semaphore_signal(barrier, inc=1, device_id=p, device_id_type=MESH)
 
     rows = tok_ref.shape[0]
 
     def choose():
+        for c in tables:
+            c.wait()
         lane = lax.broadcasted_iota(jnp.int32, (rows, LANES), 1)
         place = jnp.bitwise_and(lane, 15)
         plane = jnp.bitwise_xor(z, jnp.bitwise_and(lax.shift_right_logical(lane, 4), 3))
@@ -206,11 +221,11 @@
         w_low[...] = (weights - high.astype(f32)).astype(bf16)
 
     def load():
-        for c in loads:
+        for c in loads[:4]:
             c.start()
 
     attend(
-        load, choose, len_ref, tok_hbm, key_hbm, value_hbm, gate_hbm, mix_hbm, wq_hbm, wk_hbm, wv_hbm, wf_hbm, wo_hbm,
+        first_loads, load, choose, len_ref, tok_hbm, key_hbm, value_hbm, gate_hbm, mix_hbm, wq_hbm, wk_hbm, wv_hbm, wf_hbm, wo_hbm,
         part_ref, *scratch[:ATTEND_SCRATCH],
     )
     loads[4].wait()
@@ -361,26 +376,29 @@
     for d in (1, 3):
         c_xc[d].wait_recv()
     crossed = ys[0, 2:4].astype(f32) + rxc[1].astype(f32) + rxc[3].astype(f32)
-    c_out[...] = crossed[1].astype(bf16)
-    c_rc = send(c_out, rc, y_peer)
     spread = lambda v: lax.dot_general(
         tight, v.astype(bf16), (((0,), (0,)), ((), ())), preferred_element_type=f32
     ).astype(bf16).reshape(4, 16, HALF)
+    er[1] = spread(crossed[0])
+    er[2] = spread(crossed[1])
+    order = (2, 1, 3, 0)
+    c_r = [send(er.at[1, k], rb.at[1, k], z_cross[k]) for k in order]
+    c_r += [send(er.at[2, k], rb.at[2, k], z_far[k]) for k in order]
     for d in (1, 3):
         c_xo[d].wait_recv()
     own = zs_out[0].astype(f32) + rxo[1].astype(f32) + rxo[3].astype(f32)
     er[0] = spread(own)
     rb[0, 0] = er[0, 0]
-    c_r0 = {k: send(er.at[0, k], rb.at[0, k], z_peer[k]) for k in near}
-    c_rc.wait_recv()
-    er[1] = spread(crossed[0] + rc[...].astype(f32))
-    c_r1 = {k: send(er.at[1, k], rb.at[1, k], z_cross[k]) for k in (2, 1, 3, 0)}
-    for k in near:
-        c_r0[k].wait_recv()
-    for k in (2, 1, 3, 0):
-        c_r1[k].wait_recv()
-    returned = rb[...].reshape(LANES, HALF)
-    mixture = res[t].astype(f32) + dot(w_high[...], returned) + dot(w_low[...], returned)
+    c_r += [send(er.at[0, k], rb.at[0, k], z_peer[k]) for k in order[:3]]
+    mixture = res[t].astype(f32)
+    for c in c_r[:8]:
+        c.wait_recv()
+    weigh = lambda a, v: dot(w_high[:, a : a + 64], v) + dot(w_low[:, a : a + 64], v)
+    for i in (1, 2):
+        mixture = mixture + weigh(64, rb[i].reshape(64, HALF))
+    for c in c_r[8:]:
+        c.wait_recv()
+    mixture = mixture + weigh(0, rb[0].reshape(64, HALF))
     fo[t] = mixture.astype(bf16)
     c_fo = send(fo.at[t], fo.at[t], partner)
     c_fo.wait_recv()
@@ -398,14 +416,13 @@
     f32, bf16 = jnp.float32, jnp.bfloat16
     any_space = pl.BlockSpec(memory_space=pl.ANY)
     vmem = pl.BlockSpec(memory_space=pltpu.VMEM)
-    smem = pl.BlockSpec(memory_space=pltpu.SMEM)
     blocks = lambda *s: pltpu.VMEM((*s, BLOCK, HALF), bf16)
     heads = pltpu.VMEM((SEQS * HEADS_HERE, LANES), f32)
     forget = forget_weight.T
     return pl.pallas_call(
         layer_kernel,
-        out_shape=jax.ShapeDtypeStruct((rows, width), bf16),
-        in_specs=[smem] + [any_space] * 11 + [vmem] * 2 + [any_space] * 3,
+        out_shape=pltpu.VMEM((rows, width), bf16),
+        in_specs=[any_space] * 17,
         out_specs=vmem,
         scratch_shapes=[
             pltpu.VMEM((rows, width), bf16),
@@ -426,6 +443,9 @@
             heads,
             pltpu.SemaphoreType.DMA((7,)),
             pltpu.SemaphoreType.DMA((3, KV_BLOCKS)),
+            pltpu.SMEM((rows,), jnp.int32),
+            pltpu.VMEM((2, rows), jnp.int32),
+            pltpu.VMEM((2, rows), f32),
             pltpu.VMEM((1, width), f32),
             pltpu.VMEM(expert_gate.shape, bf16),
             pltpu.VMEM(expert_up.shape, bf16),
@@ -447,17 +467,15 @@
             blocks(4),
             blocks(4),
             blocks(4, 2),
-            blocks(),
-            blocks(),
-            pltpu.VMEM((2, 4, 16, HALF), bf16),
-            pltpu.VMEM((2, 4, 16, HALF), bf16),
+            pltpu.VMEM((3, 4, 16, HALF), bf16),
+            pltpu.VMEM((3, 4, 16, HALF), bf16),
             pltpu.VMEM((2, rows, HALF), bf16),
             pltpu.VMEM((4, CHUNK, expert_gate.shape[1]), bf16),
             pltpu.VMEM((4, 2, BLOCK, HALF // 2), bf16),
             pltpu.VMEM((4, BLOCK, HALF // 2), bf16),
-            pltpu.SemaphoreType.DMA((5,)),
-            pltpu.SemaphoreType.DMA((72,)),
-            pltpu.SemaphoreType.DMA((72,)),
+            pltpu.SemaphoreType.DMA((8,)),
+            pltpu.SemaphoreType.DMA((80,)),
+            pltpu.SemaphoreType.DMA((80,)),
         ],
         compiler_params=pltpu.CompilerParams(
             collective_id=0, has_side_effects=True, vmem_limit_bytes=60 * 1024 * 1024

time: 67.5 us -> 63.9 us (0.947)
  Pallas kernels: 65.8 us -> 63.1 us
  local copies, waits for them, and re-layouts: 1.57 us -> 0.66 us
    pallas_call x1, Pallas kernels: 65.8 us -> 63.1 us  [on_device(): pl.pallas_call(layer_kernel, out_shape=pltpu.VMEM((rows, width), bf16), i...]
    unnamed x1, local copies, waits for them, and re-layouts: 1.57 us -> 0.66 us
where the time goes in v6:
time: 63.9 us; the launch traced here: 63.8 us
  Pallas kernels  63.1 us (99%)
  local copies, waits for them, and re-layouts  0.66 us (1%)
    pallas_call x1, Pallas kernels, on_device(): pl.pallas_call(layer_kernel, out_shape=pltpu.VMEM((rows, width), bf16), i...  63.1 us

profile of v6, /device:TPU:1, one launch (start us, length us, event | category | flops | bytes accessed | tf_op | source)
XLA Modules:
  0.0 63.8 jit_solution(12394760488207536576)
XLA Ops:
  0.0 63.1 %decode_layer.1 = bf16[32,2048]{1,0:T(8,128)(2,1)S(1)} custom-call(s32[32]{0:T(128)} %len_hbm.1, bf16[32,2048]{1,0:T(8,128)(2,1)} %tok_hbm.1, bf16[32,1024,128]{2,1,0:T(8,128)(2,1)} %key_hbm.1, bf16[32,1024,128]{2,1,0:T(8,128)(2,1)} %value_hbm.1, f32[32,8,1024]{2,1,0:T(8,128)} %gate_hbm.1, f32[1,2048]{1,0:T(1,128)} %bitcast.6, bf16[2048,512]{1,0:T(8,128)(2,1)} %wq_hbm.1, ...), custom_call_target="tpu_custom_call" | custom-call | flops 5500000256 | bytes 30000000 | tf_op jit(solution)/shard_map/decode_layer/pallas_call | solution.py:422
  63.2 0.7 %copy.19 = bf16[32,2048]{1,0:T(8,128)(2,1)} copy(bf16[32,2048]{1,0:T(8,128)(2,1)S(1)} %decode_layer.1) | data formatting | bytes 262144

commit v7 on v6

--- a/solution.py
+++ b/solution.py
@@ -124,6 +124,8 @@
 HALF = 1024
 BLOCK = 48
 CHUNK = 4 * BLOCK
+SEND_SLOTS = 34
+COPIES = 66
 
 
 ATTEND_SCRATCH = 17
@@ -181,8 +183,10 @@
     def send(src, dst, device):
         i = count[0]
         count[0] += 1
+        if i >= SEND_SLOTS:
+            started[i - SEND_SLOTS].wait_send()
         c = pltpu.make_async_remote_copy(
-            src_ref=src, dst_ref=dst, send_sem=ss.at[i], recv_sem=rs.at[i], device_id=device, device_id_type=MESH
+            src_ref=src, dst_ref=dst, send_sem=ss.at[i % SEND_SLOTS], recv_sem=rs.at[i], device_id=device, device_id_type=MESH
         )
         c.start()
         started.append(c)
@@ -355,17 +359,19 @@
 
     compute(0)
     arrive(2)
-    compute(2)
+    hide(2)
+    arrive(1)
+    down(2)
     finish(0)
-    arrive(1)
     hide(1)
     finish(2)
+    arrive(3)
     down(1)
-    arrive(3)
-    compute(3)
+    hide(3)
+    finish(1)
+    down(3)
+    across(1)
     second(2)
-    finish(1)
-    across(1)
     finish(3)
     across(3)
     second(1)
@@ -404,7 +410,7 @@
     c_fo.wait_recv()
     out_ref[:, 0:HALF] = fo[0]
     out_ref[:, HALF : 2 * HALF] = fo[1]
-    for c in started:
+    for c in started[-SEND_SLOTS:]:
         c.wait_send()
 
 
@@ -474,8 +480,8 @@
             pltpu.VMEM((4, 2, BLOCK, HALF // 2), bf16),
             pltpu.VMEM((4, BLOCK, HALF // 2), bf16),
             pltpu.SemaphoreType.DMA((8,)),
-            pltpu.SemaphoreType.DMA((80,)),
-            pltpu.SemaphoreType.DMA((80,)),
+            pltpu.SemaphoreType.DMA((SEND_SLOTS,)),
+            pltpu.SemaphoreType.DMA((COPIES,)),
         ],
         compiler_params=pltpu.CompilerParams(
             collective_id=0, has_side_effects=True, vmem_limit_bytes=60 * 1024 * 1024

time: 63.9 us -> 62.2 us (0.973)
  Pallas kernels: 63.1 us -> 61.5 us
    pallas_call x1, Pallas kernels: 63.1 us -> 61.5 us  [on_device(): pl.pallas_call(layer_kernel, out_shape=pltpu.VMEM((rows, width), bf16), i...]
where the time goes in v7:
time: 62.2 us; the launch traced here: 62.1 us
  Pallas kernels  61.5 us (99%)
  local copies, waits for them, and re-layouts  0.66 us (1%)
    pallas_call x1, Pallas kernels, on_device(): pl.pallas_call(layer_kernel, out_shape=pltpu.VMEM((rows, width), bf16), i...  61.5 us

profile of v7, /device:TPU:1, one launch (start us, length us, event | category | flops | bytes accessed | tf_op | source)
XLA Modules:
  0.0 62.1 jit_solution(12558167958952142370)
XLA Ops:
  0.0 61.5 %decode_layer.1 = bf16[32,2048]{1,0:T(8,128)(2,1)S(1)} custom-call(s32[32]{0:T(128)} %len_hbm.1, bf16[32,2048]{1,0:T(8,128)(2,1)} %tok_hbm.1, bf16[32,1024,128]{2,1,0:T(8,128)(2,1)} %key_hbm.1, bf16[32,1024,128]{2,1,0:T(8,128)(2,1)} %value_hbm.1, f32[32,8,1024]{2,1,0:T(8,128)} %gate_hbm.1, f32[1,2048]{1,0:T(1,128)} %bitcast.6, bf16[2048,512]{1,0:T(8,128)(2,1)} %wq_hbm.1, ...), custom_call_target="tpu_custom_call" | custom-call | flops 5500000256 | bytes 30000000 | tf_op jit(solution)/shard_map/decode_layer/pallas_call | solution.py:428
  61.5 0.7 %copy.19 = bf16[32,2048]{1,0:T(8,128)(2,1)} copy(bf16[32,2048]{1,0:T(8,128)(2,1)S(1)} %decode_layer.1) | data formatting | bytes 262144

commit v8 on v7

--- a/solution.py
+++ b/solution.py
@@ -124,7 +124,7 @@
 HALF = 1024
 BLOCK = 48
 CHUNK = 4 * BLOCK
-SEND_SLOTS = 34
+SEND_SLOTS = 26
 COPIES = 66
 
 
@@ -248,8 +248,8 @@
         picks[...], xe[t], (((0,), (0,)), ((), ())), preferred_element_type=f32
     ).astype(bf16).reshape(8, 16, HALF)
     sb[0, 0] = pk[0]
-    c_s0 = {k: send(pk.at[k], sb.at[0, k], z_peer[k]) for k in near}
-    c_s1 = {k: send(pk.at[4 + k], sb.at[1, k], z_cross[k]) for k in (0, 1, 3, 2)}
+    c_s0 = {k: send(pk.at[k], sb.at[0, k], z_peer[k]) for k in (2, 1, 3)}
+    c_s1 = {k: send(pk.at[4 + k], sb.at[1, k], z_cross[k]) for k in (2, 1, 3, 0)}
     r_i = lax.broadcasted_iota(jnp.int32, (BLOCK, 64), 0)
     c_i = lax.broadcasted_iota(jnp.int32, (BLOCK, 64), 1)
     r_k = lax.shift_right_logical(r_i * 43, 9)
@@ -388,8 +388,10 @@
     er[1] = spread(crossed[0])
     er[2] = spread(crossed[1])
     order = (2, 1, 3, 0)
-    c_r = [send(er.at[1, k], rb.at[1, k], z_cross[k]) for k in order]
-    c_r += [send(er.at[2, k], rb.at[2, k], z_far[k]) for k in order]
+    c_r = []
+    for k in order:
+        c_r.append(send(er.at[2, k], rb.at[2, k], z_far[k]))
+        c_r.append(send(er.at[1, k], rb.at[1, k], z_cross[k]))
     for d in (1, 3):
         c_xo[d].wait_recv()
     own = zs_out[0].astype(f32) + rxo[1].astype(f32) + rxo[3].astype(f32)

time: 62.2 us -> 61.4 us (0.987)
  Pallas kernels: 61.5 us -> 60.6 us
    pallas_call x1, Pallas kernels: 61.5 us -> 60.6 us  [on_device(): pl.pallas_call(layer_kernel, out_shape=pltpu.VMEM((rows, width), bf16), i...]
where the time goes in v8:
time: 61.4 us; the launch traced here: 61.3 us
  Pallas kernels  60.6 us (99%)
  local copies, waits for them, and re-layouts  0.66 us (1%)
    pallas_call x1, Pallas kernels, on_device(): pl.pallas_call(layer_kernel, out_shape=pltpu.VMEM((rows, width), bf16), i...  60.6 us

profile of v8, /device:TPU:1, one launch (start us, length us, event | category | flops | bytes accessed | tf_op | source)
XLA Modules:
  0.0 61.3 jit_solution(2028458636876690434)
XLA Ops:
  0.0 60.6 %decode_layer.1 = bf16[32,2048]{1,0:T(8,128)(2,1)S(1)} custom-call(s32[32]{0:T(128)} %len_hbm.1, bf16[32,2048]{1,0:T(8,128)(2,1)} %tok_hbm.1, bf16[32,1024,128]{2,1,0:T(8,128)(2,1)} %key_hbm.1, bf16[32,1024,128]{2,1,0:T(8,128)(2,1)} %value_hbm.1, f32[32,8,1024]{2,1,0:T(8,128)} %gate_hbm.1, f32[1,2048]{1,0:T(1,128)} %bitcast.6, bf16[2048,512]{1,0:T(8,128)(2,1)} %wq_hbm.1, ...), custom_call_target="tpu_custom_call" | custom-call | flops 5500000256 | bytes 30000000 | tf_op jit(solution)/shard_map/decode_layer/pallas_call | solution.py:430
  60.6 0.7 %copy.19 = bf16[32,2048]{1,0:T(8,128)(2,1)} copy(bf16[32,2048]{1,0:T(8,128)(2,1)S(1)} %decode_layer.1) | data formatting | bytes 262144

commit v9 on v8

--- a/solution.py
+++ b/solution.py
@@ -38,13 +38,14 @@
     first()
     for c in copies[2:6]:
         c.start()
+    for c in block_copies(0):
+        c.start()
     meanwhile()
     with jax.named_scope("wait_tok"):
         copies[0].wait()
         copies[1].wait()
-    for b in range(2):
-        for c in block_copies(b):
-            c.start()
+    for c in block_copies(1):
+        c.start()
     ni = rms(tok[...].astype(jnp.float32), gain[...]).astype(jnp.bfloat16)
     lane = lax.broadcasted_iota(jnp.int32, (SEQS, LANES), 1)
     left = lane < 64

time: 61.4 us -> 60.6 us (0.987)
  Pallas kernels: 60.6 us -> 59.8 us
    pallas_call x1, Pallas kernels: 60.6 us -> 59.8 us  [on_device(): pl.pallas_call(layer_kernel, out_shape=pltpu.VMEM((rows, width), bf16), i...]
where the time goes in v9:
time: 60.6 us; the launch traced here: 60.5 us
  Pallas kernels  59.8 us (99%)
  local copies, waits for them, and re-layouts  0.66 us (1%)
    pallas_call x1, Pallas kernels, on_device(): pl.pallas_call(layer_kernel, out_shape=pltpu.VMEM((rows, width), bf16), i...  59.8 us

profile of v9, /device:TPU:1, one launch (start us, length us, event | category | flops | bytes accessed | tf_op | source)
XLA Modules:
  0.0 60.5 jit_solution(14505120976189024736)
XLA Ops:
  0.0 59.8 %decode_layer.1 = bf16[32,2048]{1,0:T(8,128)(2,1)S(1)} custom-call(s32[32]{0:T(128)} %len_hbm.1, bf16[32,2048]{1,0:T(8,128)(2,1)} %tok_hbm.1, bf16[32,1024,128]{2,1,0:T(8,128)(2,1)} %key_hbm.1, bf16[32,1024,128]{2,1,0:T(8,128)(2,1)} %value_hbm.1, f32[32,8,1024]{2,1,0:T(8,128)} %gate_hbm.1, f32[1,2048]{1,0:T(1,128)} %bitcast.6, bf16[2048,512]{1,0:T(8,128)(2,1)} %wq_hbm.1, ...), custom_call_target="tpu_custom_call" | custom-call | flops 5500000256 | bytes 30000000 | tf_op jit(solution)/shard_map/decode_layer/pallas_call | solution.py:431
  59.9 0.7 %copy.19 = bf16[32,2048]{1,0:T(8,128)(2,1)} copy(bf16[32,2048]{1,0:T(8,128)(2,1)S(1)} %decode_layer.1) | data formatting | bytes 262144
